TPU v7x, 128 devices: a whole 4x4x4 slice. The times are simulated.
128 devices in a mesh: sp: 16 (over z, y), dp: 8 (over x, core).
Axes of the slice: x: 4, y: 4, z: 4, core: 2. Of those that a mesh axis runs over, the one named last changes fastest.
Arguments:
- residual: bfloat16 [8, 2048, 2048], P('dp', 'sp'), may hold values from -6 to 6
- query: bfloat16 [8, 2048, 16, 128], P('dp', 'sp'), may hold values from -6 to 6
- key_value: bfloat16 [8, 2048, 16, 128], P('dp', 'sp'), may hold values from -6 to 6
- out_weight: bfloat16 [2048, 2048], P(None, 'dp'), may hold values from -0.125 to 0.125
- norm_gain: float32 [2048], replicated, may hold values from 0.1 to 1.9
- query_gain: float32 [64], replicated, may hold values from 1.5 to 4.5
- key_gain: float32 [64], replicated, may hold values from 1.5 to 4.5
- route_ids: int32 [8, 2048, 4], P('dp', 'sp'), may hold values from 0 to 127, all different within a row; in each aligned block of 128 rows (0 to 127, 128 to 255, ..., all dimensions but the last counted through in order) at most 6 rows name the same one
- route_weights: float32 [8, 2048, 4], P('dp', 'sp'), may hold values from 0.2 to 1
- shared_gate: bfloat16 [2048, 512], replicated, may hold values from -0.125 to 0.125
- shared_up: bfloat16 [2048, 512], replicated, may hold values from -0.125 to 0.125
- shared_down: bfloat16 [512, 2048], replicated, may hold values from -0.25 to 0.25
- expert_gate: bfloat16 [128, 2048, 512], P(('sp', 'dp')), may hold values from -0.125 to 0.125
- expert_up: bfloat16 [128, 2048, 512], P(('sp', 'dp')), may hold values from -0.125 to 0.125
- expert_down: bfloat16 [128, 512, 2048], P(('sp', 'dp')), may hold values from -0.25 to 0.25
Outputs:
- result: bfloat16 [8, 2048, 2048], P('dp', 'sp')
Inputs may be any that keep to these rules, and one draw needn't show every extreme that they name: `route_ids`: each row names 4 different experts. Among the rows of one device no expert is named more than 6 times, a bound that some block reaches.
All inputs are finite; a program needn't handle non-finite values.
Results may differ from a plain program's by a relative error of at most 0.014.
The roundings to bfloat16 on the way count: a program that leaves them out, or rounds other values in their place, can miss the bound.
Values may be sent and summed in bfloat16 or wider, within the bound.
A program may use at most 128 MiB of HBM per device.

v0:
```python
import jax
import jax.numpy as jnp
from jax import lax
from jax.sharding import PartitionSpec as P

GRID_W = 64


norm_eps = 1e-06
rope_theta = 10000.0
routed_scale = 2.5


def rotate_half(values, position, half_width):
    inverse_freq = rope_theta ** (-jnp.arange(0, half_width, 2, dtype=jnp.float32) / half_width)
    angles = position.astype(jnp.float32)[:, None] * inverse_freq[None, :]
    angles = jnp.concatenate([angles, angles], axis=-1)
    cosine = jnp.cos(angles)[:, None, :]
    sine_part = jnp.sin(angles)[:, None, :]
    first_half, second = jnp.split(values, 2, axis=-1)
    turned = jnp.concatenate([-second, first_half], axis=-1)
    return values * cosine + turned * sine_part


def prepare(values, gain_vector, grid_row, grid_col):
    head_dim = values.shape[-1]
    floats = values.astype(jnp.float32)
    normed = floats * lax.rsqrt(jnp.mean(floats * floats, axis=-1, keepdims=True) + norm_eps)
    normed = normed * gain_vector
    half_width = head_dim // 2
    turned = jnp.concatenate(
        [
            rotate_half(normed[..., :half_width], grid_row, half_width),
            rotate_half(normed[..., half_width:], grid_col, half_width),
        ],
        axis=-1,
    )
    return turned.astype(jnp.bfloat16)


def attend(queries, key_rows, values):
    length, groups, repeats, head_dim = queries.shape
    block_rows = min(512, length)
    score_scale = head_dim ** (-0.5)

    def one_block(query_block):
        scores = (
            jnp.einsum("qgrd,kgd->grqk", query_block, key_rows, preferred_element_type=jnp.float32)
            * score_scale
        )
        row_max = jnp.max(scores, axis=-1, keepdims=True)
        weights = jnp.exp(scores - row_max)
        row_total = jnp.sum(weights, axis=-1, keepdims=True)
        rounded = weights.astype(jnp.bfloat16)
        mixed = (
            jnp.einsum("grqk,kgd->grqd", rounded, values, preferred_element_type=jnp.float32)
            / row_total
        )
        return jnp.transpose(mixed, (2, 0, 1, 3)).astype(jnp.bfloat16)

    blocks = queries.reshape(length // block_rows, block_rows, groups, repeats, head_dim)
    return lax.map(one_block, blocks).reshape(length, groups * repeats * head_dim)


def swiglu(row_block, gate_weight, up_weight, down_weight):
    gate_part = jnp.dot(row_block, gate_weight, preferred_element_type=jnp.float32)
    up_part = jnp.dot(row_block, up_weight, preferred_element_type=jnp.float32)
    hidden = (jax.nn.silu(gate_part) * up_part).astype(jnp.bfloat16)
    return jnp.dot(hidden, down_weight, preferred_element_type=jnp.float32)


def per_device(
    residual,
    query,
    key_value,
    out_weight,
    norm_gain,
    query_gain,
    key_gain,
    route_ids,
    route_weights,
    shared_gate,
    shared_up,
    shared_down,
    expert_gate,
    expert_up,
    expert_down,
):
    tokens = residual.shape[1]
    model_width = residual.shape[2]
    head_dim = key_value.shape[3] // 2
    head_rows, pair_rows = (
        lax.all_to_all(query, "sp", split_axis=2, concat_axis=1, tiled=True),
        lax.all_to_all(key_value, "sp", split_axis=2, concat_axis=1, tiled=True),
    )
    length = head_rows.shape[1]
    kv_local = head_rows.shape[2]
    repeats = head_rows.shape[3] // head_dim
    position = jnp.arange(length, dtype=jnp.int32)
    grid_row = position // GRID_W
    grid_col = position % GRID_W
    queries = prepare(
        head_rows[0].reshape(length, kv_local * repeats, head_dim), query_gain, grid_row, grid_col
    )
    queries = queries.reshape(length, kv_local, repeats, head_dim)
    key_rows = prepare(pair_rows[0][..., :head_dim], key_gain, grid_row, grid_col)
    values = pair_rows[0][..., head_dim:]
    attention = attend(queries, key_rows, values)
    returned_heads = lax.all_to_all(
        attention.reshape(1, length, kv_local, repeats * head_dim),
        "sp",
        split_axis=1,
        concat_axis=2,
        tiled=True,
    )
    flat_rows = returned_heads.reshape(tokens, -1)
    projected = jnp.dot(
        flat_rows,
        lax.all_gather(out_weight, "dp", axis=1, tiled=True),
        preferred_element_type=jnp.float32,
    )
    mixed = residual[0].astype(jnp.float32) + projected
    normed = mixed * lax.rsqrt(jnp.mean(mixed * mixed, axis=-1, keepdims=True) + norm_eps)
    normed = (normed * norm_gain).astype(jnp.bfloat16)
    shared = swiglu(normed, shared_gate, shared_up, shared_down)
    local_experts = expert_gate.shape[0]
    experts = local_experts * lax.axis_size(("sp", "dp"))
    top_count = route_ids.shape[2]
    slot_count = max(2, 3 * tokens * top_count // (2 * experts))
    route_list = route_ids[0].reshape(-1)
    raw_weights = route_weights[0]
    gate_values = (
        raw_weights / jnp.sum(raw_weights, axis=-1, keepdims=True) * routed_scale
    ).reshape(-1)
    hit_table = (route_list[:, None] == jnp.arange(experts, dtype=jnp.int32)[None, :]).astype(
        jnp.int32
    )
    slot_rank = jnp.sum((jnp.cumsum(hit_table, axis=0) - hit_table) * hit_table, axis=1)
    slot_place = route_list * slot_count + slot_rank
    outgoing = jnp.zeros((experts * slot_count, model_width), jnp.bfloat16)
    outgoing = outgoing.at[slot_place].set(jnp.repeat(normed, top_count, axis=0))
    outgoing = outgoing.reshape(experts, slot_count, model_width)
    arrived = lax.all_to_all(outgoing, ("sp", "dp"), split_axis=0, concat_axis=0, tiled=True)
    sources = arrived.shape[0] // local_experts
    slot_width = arrived.shape[1]
    grouped = arrived.reshape(sources, local_experts, slot_width, model_width)
    row_block = grouped[:, 0].reshape(-1, model_width)
    output = swiglu(row_block, expert_gate[0], expert_up[0], expert_down[0])
    results = [output.astype(jnp.bfloat16).reshape(sources, slot_width, model_width)]
    returned = lax.all_to_all(
        jnp.stack(results, axis=1).reshape(arrived.shape),
        ("sp", "dp"),
        split_axis=0,
        concat_axis=0,
        tiled=True,
    )
    gathered = returned.reshape(experts * slot_count, model_width)[slot_place]
    routed = jnp.sum(
        (gathered.astype(jnp.float32) * gate_values[:, None]).reshape(
            tokens, top_count, model_width
        ),
        axis=1,
    )
    combined = (mixed + shared + routed).astype(jnp.bfloat16)
    return combined.reshape(1, tokens, model_width)


def solution(mesh):
    in_specs = (
        P("dp", "sp", None),
        P("dp", "sp", None, None),
        P("dp", "sp", None, None),
        P(None, "dp"),
        P(),
        P(),
        P(),
        P("dp", "sp", None),
        P("dp", "sp", None),
        P(),
        P(),
        P(),
        P(("sp", "dp"), None, None),
        P(("sp", "dp"), None, None),
        P(("sp", "dp"), None, None),
    )
    out_specs = P("dp", "sp", None)
    return jax.shard_map(
        per_device, mesh=mesh, in_specs=in_specs, out_specs=out_specs, check_vma=False
    )
```

profile of v0, /device:TPU:1, one launch (start us, length us, event | category | flops | bytes accessed | tf_op | source)
XLA Modules:
  0.0 317.5 jit_solution(13781153775951942175)
XLA Ops:
  9.3 8.6 %all-to-all-start = ((bf16[1,128,16,128]{3,1,0,2:T(8,128)(2,1)}), bf16[1,128,16,128]{3,1,0,2:T(8,128)(2,1)S(1)}, u32[]{:S(2)}, u32[]{:S(2)}) async-start(bf16[1,128,16,128]{3,1,0,2:T(8,128)(2,1)} %copy.34), calls=%async_computation | async-start | bytes 1048576 | tf_op jit(solution)/shard_map/all_to_all | solution.py:93
  21.2 2.6 fusion.51
  23.7 4.6 %all-to-all-done = bf16[1,128,16,128]{3,1,0,2:T(8,128)(2,1)S(1)} async-done(((bf16[1,128,16,128]{3,1,0,2:T(8,128)(2,1)}), bf16[1,128,16,128]{3,1,0,2:T(8,128)(2,1)S(1)}, u32[]{:S(2)}, u32[]{:S(2)}) %all-to-all-start) | async-done | bytes 524320 | tf_op jit(solution)/shard_map/all_to_all | solution.py:93
  29.1 4.2 %all-to-all-start.1 = ((bf16[1,128,16,128]{3,1,0,2:T(8,128)(2,1)}), bf16[1,128,16,128]{3,1,0,2:T(8,128)(2,1)}, u32[]{:S(2)}, u32[]{:S(2)}) async-start(bf16[1,128,16,128]{3,1,0,2:T(8,128)(2,1)} %copy.36), calls=%async_computation.1 | async-start | bytes 1048576 | tf_op jit(solution)/shard_map/all_to_all | solution.py:94
  39.5 3.5 %all-to-all-done.1 = bf16[1,128,16,128]{3,1,0,2:T(8,128)(2,1)} async-done(((bf16[1,128,16,128]{3,1,0,2:T(8,128)(2,1)}), bf16[1,128,16,128]{3,1,0,2:T(8,128)(2,1)}, u32[]{:S(2)}, u32[]{:S(2)}) %all-to-all-start.1) | async-done | bytes 524320 | tf_op jit(solution)/shard_map/all_to_all | solution.py:94
  43.0 2.3 fusion.85
  47.6 3.1 fusion.49
  50.8 18.8 %while.10 = (s32[]{:T(128)}, bf16[4,512,1,2,64]{1,4,3,2,0:T(8,128)(2,1)S(1)}, bf16[4,512,1,2,64]{1,4,3,2,0:T(8,128)(2,1)S(1)}, bf16[2048,1,64]{0,2,1:T(8,128)(2,1)S(1)}, bf16[2048,1,64]{0,2,1:T(8,128)(2,1)}, /*index=5*/s32[]{:T(128)}) while((s32[]{:T(128)}, bf16[4,512,1,2,64]{1,4,3,2,0:T(8,128)(2,1)S(1)}, ...), condition=%wide.region_5.6_spmd, body=%wide.region_2.5_spmd.sunk | while | flops 553777152 | bytes 27021416 | solution.py:62
  71.7 4.3 %reshape.587 = bf16[1,2048,1,128]{3,2,0,1:T(2,128)(2,1)S(1)} reshape(bf16[4,512,1,2,64]{4,3,1,0,2:T(2,128)(2,1)} %copy.49) | data formatting | bytes 1048576 | tf_op jit(solution)/shard_map/reshape;reshape | solution.py:110
  76.5 12.5 %reduce.4 = bf16[2048,128]{1,0:T(8,128)(2,1)} reduce(bf16[2048,1,1,128]{3,2,1,0:T(2,128)(2,1)S(1)} %bitcast.151, bf16[]{:T(256)} %broadcast.319), dimensions={1,2}, to_apply=%bitcast.116.reduce_sub_computation | reduce | bytes 1048578
  90.9 4.2 %all-to-all-start.2 = ((bf16[16,2,8192]{2,1,0:T(2,128)(2,1)}), bf16[16,2,8192]{2,1,0:T(2,128)(2,1)}, u32[]{:S(2)}, u32[]{:S(2)}) async-start(bf16[16,2,8192]{2,1,0:T(2,128)(2,1)} %reshape.590), calls=%async_computation.2 | async-start | bytes 1048576 | tf_op jit(solution)/shard_map/all_to_all | solution.py:109
  95.6 8.5 %all-to-all-done.2 = bf16[16,2,8192]{2,1,0:T(2,128)(2,1)} async-done(((bf16[16,2,8192]{2,1,0:T(2,128)(2,1)}), bf16[16,2,8192]{2,1,0:T(2,128)(2,1)}, u32[]{:S(2)}, u32[]{:S(2)}) %all-to-all-start.2) | async-done | bytes 524320 | tf_op jit(solution)/shard_map/all_to_all | solution.py:109
  104.2 2.2 reshape.591
  107.2 2.1 copy.42
  109.3 4.9 %multiply_reduce_fusion.1 = (f32[128]{0:T(128)S(1)}, f32[128,2048]{1,0:T(8,128)S(1)}) fusion(bf16[128,2048]{0,1:T(8,128)(2,1)} %bitcast.152, bf16[2048,2048]{1,0:T(8,128)(2,1)} %all-gather.2.cloned.1.call-done, bf16[1,128,2048]{2,1,0:T(8,128)(2,1)} %param.17), kind=kOutput, calls=%fused_computation.39 | convolution fusion | flops 1074790272 | bytes 10486272 | tf_op jit(solution)/shard_map/dot_general | solution.py:117
  115.3 2.4 broadcast_in_dim.11
  117.6 3.9 %reshape.581 = bf16[512,2048]{1,0:T(8,128)(2,1)} reshape(bf16[128,4,2048]{2,1,0:T(4,128)(2,1)} %broadcast_in_dim.11) | data formatting | bytes 4194304 | tf_op jit(solution)/shard_map/reshape | solution.py:141
  121.6 6.7 %scatter_custom_fusion = bf16[768,2048]{1,0:T(8,128)(2,1)} fusion(s32[512]{0:T(512)S(1)} %bitcast.158, bf16[512,2048]{1,0:T(8,128)(2,1)} %reshape.581, bf16[]{:T(256)} %constant.70.clone.1), kind=kCustom, calls=%fused_computation.33 | custom fusion | bytes 3146240 | tf_op jit(solution)/shard_map/scatter | solution.py:141
  128.3 6.2 %reshape.562 = bf16[128,6,2048]{2,1,0:T(8,128)(2,1)} reshape(bf16[768,2048]{1,0:T(8,128)(2,1)} %scatter_custom_fusion) | data formatting | bytes 6291456 | tf_op jit(solution)/shard_map/reshape | solution.py:142
  134.5 62.2 %all_to_all.49 = bf16[128,6,2048]{2,1,0:T(8,128)(2,1)} all-to-all(bf16[128,6,2048]{2,1,0:T(8,128)(2,1)} %reshape.562), channel_id=1, replica_groups=mesh['sp'=16,'dp'=8] {'sp','dp'}, dimensions={0} | all-to-all | bytes 6291456 | tf_op jit(solution)/shard_map/all_to_all | solution.py:143
  196.8 6.3 %reshape_squeeze_reshape.3 = bf16[768,2048]{1,0:T(8,128)(2,1)} reshape(bf16[128,6,2048]{2,1,0:T(8,128)(2,1)} %all_to_all.49) | data formatting | bytes 6291456 | tf_op jit(solution)/shard_map/reshape;squeeze;reshape | solution.py:147
  203.1 5.5 %fusion.31 = f32[768,512]{1,0:T(8,128)} fusion(bf16[768,2048]{1,0:T(8,128)(2,1)} %reshape_squeeze_reshape.3, bf16[1,2048,512]{2,1,0:T(8,128)(2,1)} %param.29), kind=kOutput, calls=%fused_computation.30 | convolution fusion | flops 1610612736 | bytes 6815744 | tf_op jit(solution)/shard_map/dot_general | solution.py:66
  208.6 8.2 %convolution_convert_fusion = bf16[768,2048]{1,0:T(8,128)(2,1)} fusion(bf16[1,512,2048]{2,1,0:T(8,128)(2,1)S(1)} %copy-done, f32[768,512]{1,0:T(8,128)} %fusion.31, bf16[768,2048]{1,0:T(8,128)(2,1)} %reshape_squeeze_reshape.3, bf16[1,2048,512]{2,1,0:T(8,128)(2,1)} %param.30), kind=kOutput, calls=%fused_computation.21 | convolution fusion | flops 3225157632 | bytes 12058624 | tf_op jit(solution)/shard_map/dot_general | solution.py:69
  216.7 6.3 %reshape_stack_reshape.3 = bf16[128,6,2048]{2,1,0:T(8,128)(2,1)} reshape(bf16[768,2048]{1,0:T(8,128)(2,1)} %convolution_convert_fusion) | data formatting | bytes 6291456 | tf_op jit(solution)/shard_map/reshape;stack;reshape | solution.py:151
  223.0 5.7 %all-to-all-start.4 = ((bf16[128,6,2048]{2,1,0:T(8,128)(2,1)}), bf16[128,6,2048]{2,1,0:T(8,128)(2,1)}, u32[]{:S(2)}, u32[]{:S(2)}) async-start(bf16[128,6,2048]{2,1,0:T(8,128)(2,1)} %reshape_stack_reshape.3), calls=%async_computation.4 | async-start | bytes 8388608 | tf_op jit(solution)/shard_map/all_to_all | solution.py:150
  228.8 2.2 fusion.86
  231.0 50.3 %all-to-all-done.4 = bf16[128,6,2048]{2,1,0:T(8,128)(2,1)} async-done(((bf16[128,6,2048]{2,1,0:T(8,128)(2,1)}), bf16[128,6,2048]{2,1,0:T(8,128)(2,1)}, u32[]{:S(2)}, u32[]{:S(2)}) %all-to-all-start.4) | async-done | bytes 3145760 | tf_op jit(solution)/shard_map/all_to_all | solution.py:150
  281.4 6.3 %reshape.563 = bf16[768,2048]{1,0:T(8,128)(2,1)} reshape(bf16[128,6,2048]{2,1,0:T(8,128)(2,1)} %all-to-all-done.4) | data formatting | bytes 6291456 | tf_op jit(solution)/shard_map/reshape | solution.py:157
  287.7 7.6 %gather_fusion = bf16[512,2048]{1,0:T(8,128)(2,1)} fusion(bf16[768,2048]{1,0:T(8,128)(2,1)} %reshape.563, s32[1024]{0:T(1024)S(1)} %pad_clamp_fusion), kind=kCustom, calls=%fused_computation | custom fusion | bytes 4196352 | tf_op jit(solution)/shard_map/gather | solution.py:157
  295.3 4.7 %reshape.567 = f32[128,4,2048]{2,1,0:T(4,128)} reshape(bf16[512,2048]{1,0:T(8,128)(2,1)} %gather_fusion) | data formatting | bytes 6291456 | tf_op jit(solution)/shard_map/convert_element_type | solution.py:159
  300.0 6.4 %multiply_reduce_fusion = f32[128,2048]{1,0:T(8,128)} fusion(f32[128,4,2048]{2,1,0:T(4,128)} %reshape.567, f32[128,4]{1,0:T(8,128)S(1)} %copy.48), kind=kLoop, calls=%fused_computation.20 | loop fusion | flops 1835008 | bytes 5244928 | tf_op jit(solution)/shard_map/reduce_sum | solution.py:158
  306.4 4.3 %fusion.27 = bf16[1,128,2048]{2,1,0:T(8,128)(2,1)} fusion(f32[128,2048]{1,0:T(8,128)} %multiply_reduce_fusion, f32[128,2048]{1,0:T(8,128)S(1)} %get-tuple-element.80, bf16[512,2048]{1,0:T(8,128)(2,1)} %param.28, bf16[128,2048]{1,0:T(8,128)(2,1)} %copy-done.1, bf16[2048,512]{1,0:T(8,128)(2,1)} %param.27, f32[128,512]{1,0:T(8,128)S(1)} %fusion.86), kind=kOutput, calls=%fused_computation.26 | convolution fusion | flops 538050560 | bytes 7602176 | tf_op jit(solution)/shard_map/dot_general | solution.py:69
  (103 shorter events, 40.8 us)
Async XLA Ops:
  6.5 202.0 %copy-start = (bf16[1,512,2048]{2,1,0:T(8,128)(2,1)S(1)}, bf16[1,512,2048]{2,1,0:T(8,128)(2,1)}, u32[]{:S(2)}) copy-start(bf16[1,512,2048]{2,1,0:T(8,128)(2,1)} %param.31) | copy-start | bytes 6291460
  6.5 11.4 %copy-start.11 = (s32[1,128,4]{1,2,0:T(4,128)S(1)}, s32[1,128,4]{1,2,0:T(4,128)}, u32[]{:S(2)}) copy-start(s32[1,128,4]{1,2,0:T(4,128)} %param.24) | copy-start | bytes 6148
  6.5 11.7 %copy-start.8 = (bf16[1,128,16,128]{3,2,1,0:T(8,128)(2,1)S(1)}, bf16[1,128,16,128]{3,2,1,0:T(8,128)(2,1)}, u32[]{:S(2)}) copy-start(bf16[1,128,16,128]{3,2,1,0:T(8,128)(2,1)} %param.19) | copy-start | bytes 1572868
  6.5 102.8 %all-gather.2.cloned.1.call-start = ((), (), s32[]{:S(2)}) async-start(), calls=%async_computation.5 | async-start | bytes 9437184 | tf_op jit(solution)/shard_map/all_gather | solution.py:119
  9.3 19.0 %all-to-all-start = ((bf16[1,128,16,128]{3,1,0,2:T(8,128)(2,1)}), bf16[1,128,16,128]{3,1,0,2:T(8,128)(2,1)S(1)}, u32[]{:S(2)}, u32[]{:S(2)}) async-start(bf16[1,128,16,128]{3,1,0,2:T(8,128)(2,1)} %copy.34), calls=%async_computation | async-start | bytes 1048576 | tf_op jit(solution)/shard_map/all_to_all | solution.py:93
  28.3 0.8 copy-start.2
  29.1 13.9 %all-to-all-start.1 = ((bf16[1,128,16,128]{3,1,0,2:T(8,128)(2,1)}), bf16[1,128,16,128]{3,1,0,2:T(8,128)(2,1)}, u32[]{:S(2)}, u32[]{:S(2)}) async-start(bf16[1,128,16,128]{3,1,0,2:T(8,128)(2,1)} %copy.36), calls=%async_computation.1 | async-start | bytes 1048576 | tf_op jit(solution)/shard_map/all_to_all | solution.py:94
  33.4 4.1 %copy-start.13 = (f32[64]{0:T(128)S(1)}, f32[64]{0:T(128)}, u32[]{:S(2)}) copy-start(f32[64]{0:T(128)} %param.22) | copy-start | bytes 772
  37.3 1.0 copy-start.3
  37.3 1.0 copy-start.4
  37.3 1.1 copy-start.5
  39.0 8.5 %copy-start.14 = (f32[64]{0:T(128)S(1)}, f32[64]{0:T(128)}, u32[]{:S(2)}) copy-start(f32[64]{0:T(128)} %param.23) | copy-start | bytes 772
  47.4 3.4 %copy-start.7 = (bf16[4,512,1,2,64]{1,4,3,2,0:T(8,128)(2,1)S(1)}, bf16[4,512,1,2,64]{1,4,3,2,0:T(8,128)(2,1)}, u32[]{:S(2)}) copy-start(bf16[4,512,1,2,64]{1,4,3,2,0:T(8,128)(2,1)} %custom-call.2) | copy-start | bytes 1572868
  52.2 1.7 copy-start.9
  56.9 1.7 copy-start.9
  61.6 1.6 copy-start.9
  66.3 1.6 copy-start.9
  71.7 23.7 %copy-start.6 = (s32[128,4,128]{0,2,1:T(8,128)S(1)}, s32[128,4,128]{0,2,1:T(8,128)}, u32[]{:S(2)}) copy-start(s32[128,4,128]{0,2,1:T(8,128)} %copy.47) | copy-start | bytes 786436
  90.9 13.2 %all-to-all-start.2 = ((bf16[16,2,8192]{2,1,0:T(2,128)(2,1)}), bf16[16,2,8192]{2,1,0:T(2,128)(2,1)}, u32[]{:S(2)}, u32[]{:S(2)}) async-start(bf16[16,2,8192]{2,1,0:T(2,128)(2,1)} %reshape.590), calls=%async_computation.2 | async-start | bytes 1048576 | tf_op jit(solution)/shard_map/all_to_all | solution.py:109
  109.3 5.0 %copy-start.10 = (f32[2048]{0:T(1024)S(1)}, f32[2048]{0:T(1024)}, u32[]{:S(2)}) copy-start(f32[2048]{0:T(1024)} %param.21) | copy-start | bytes 24580
  114.5 0.8 copy-start.1
  223.0 5.7 %copy-start.12 = (f32[1,128,4]{1,2,0:T(4,128)S(1)}, f32[1,128,4]{1,2,0:T(4,128)}, u32[]{:S(2)}) copy-start(f32[1,128,4]{1,2,0:T(4,128)} %param.25) | copy-start | bytes 6148
  223.0 58.4 %all-to-all-start.4 = ((bf16[128,6,2048]{2,1,0:T(8,128)(2,1)}), bf16[128,6,2048]{2,1,0:T(8,128)(2,1)}, u32[]{:S(2)}, u32[]{:S(2)}) async-start(bf16[128,6,2048]{2,1,0:T(8,128)(2,1)} %reshape_stack_reshape.3), calls=%async_computation.4 | async-start | bytes 8388608 | tf_op jit(solution)/shard_map/all_to_all | solution.py:150
Sparse Core Ops, SparseCore 0:
  9.0 57.0 all-gather.1
where the time goes:
time: 319 us; the launch traced here: 317 us
  local copies, waits for them, and re-layouts  78.9 us (25%)
  waiting for transfers between devices  67.6 us (21%)
  blocking collectives  62.2 us (19%)
  matrix products  37.2 us (12%)
  other arithmetic  35 us (11%)
  starting transfers between devices  22.7 us (7%)
  between operations  13.8 us (4%)
    all_to_all x1, blocking collectives, per_device(): lax.all_to_all(outgoing, ('sp', 'dp'), split_axis=0, concat_axis=0, tiled...  62.2 us
    all_to_all x1, waiting for transfers between devices, per_device(): lax.all_to_all(jnp.stack(results, axis=1).reshape(arrived.shape), ('sp',...  50.3 us
    unnamed x38, local copies, waits for them, and re-layouts  13.1 us
    unnamed x1, other arithmetic  12.5 us
    dot_general x2, matrix products, swiglu(): return jnp.dot(hidden, down_weight, preferred_element_type=jnp.float32)  12.5 us
    all_to_all x1, starting transfers between devices, per_device(): lax.all_to_all(query, 'sp', split_axis=2, concat_axis=1, tiled=True)  8.59 us
    all_to_all x1, waiting for transfers between devices, per_device(): lax.all_to_all(attention.reshape(1, length, kv_local, repeats * head_dim)...  8.51 us
    dot_general x2, matrix products, swiglu(): jnp.dot(row_block, gate_weight, preferred_element_type=jnp.float32)  7.69 us
  transfers between devices with their start and end apart: 5, of which 4 were waited for; matrix products, arithmetic and copies ran while one was open for 22% of the time, Pallas kernels for 0%

commit v1 on v0

--- a/solution.py
+++ b/solution.py
@@ -1,14 +1,239 @@
+import functools
 import jax
 import jax.numpy as jnp
 from jax import lax
+from jax.experimental import pallas as pl
+from jax.experimental.pallas import tpu as pltpu
 from jax.sharding import PartitionSpec as P
 
+MESH = pl.DeviceIdType.MESH
+N_DEV = 128
+CAP = 6
+SLOT = 8
+GROUPS = 4
+PER = N_DEV // GROUPS
 GRID_W = 64
-
-
+rope_theta = 10000.0
 norm_eps = 1e-06
-rope_theta = 10000.0
 routed_scale = 2.5
+
+
+def digits(n):
+    return n // 32, (n // 8) % 4, (n // 2) % 4, n % 2
+
+
+def shifted(me_digits, k, sign):
+    d = lax.rem(k * 37, 128)
+    out = []
+    for m, v, size in zip(me_digits, digits(d), (4, 4, 4, 2)):
+        out.append(lax.rem(m + sign * v + size, size))
+    z, y, x, c = out
+    return z * 4 + y, x * 2 + c
+
+
+def silu_mul(g, u):
+    return g / (1.0 + jnp.exp(-g)) * u
+
+
+def moe_kernel(
+    rows_ref, w_ref, res_ref, ngain_ref, ids_ref, rw_ref, sg_ref, su_ref, sd_ref, eg_ref, eu_ref, ed_ref,
+    out_ref,
+    w, sg, su, sd, eg, eu, ed, mixed, normed, g_hi, g_lo, send, recv, fout, ret, hid,
+    ld_sem, s_sem, r_sem, s2_sem, r2_sem,
+):
+    sp = lax.axis_index("sp")
+    dp = lax.axis_index("dp")
+    me = (sp // 4, lax.rem(sp, 4), dp // 2, lax.rem(dp, 2))
+
+    loads = [
+        pltpu.make_async_copy(a, b, ld_sem.at[i])
+        for i, (a, b) in enumerate(
+            [(w_ref, w), (sg_ref, sg), (su_ref, su), (sd_ref, sd), (eg_ref.at[0], eg), (eu_ref.at[0], eu), (ed_ref.at[0], ed)]
+        )
+    ]
+    for c in loads:
+        c.start()
+    barrier = pltpu.get_barrier_semaphore()
+
+    def greet(k, c):
+        pl.semaphore_signal(barrier, inc=1, device_id=shifted(me, k, 1), device_id_type=MESH)
+        return c
+
+    lax.fori_loop(1, N_DEV, greet, 0)
+
+    lane = lax.broadcasted_iota(jnp.int32, (128, 128), 1)
+    row = lax.broadcasted_iota(jnp.int32, (128, 128), 0)
+    raw = rw_ref[...]
+    gates = raw / jnp.sum(raw, axis=1, keepdims=True) * routed_scale
+    ids = ids_ref[...]
+    hit = jnp.zeros((128, 128), jnp.float32)
+    gate = jnp.zeros((128, 128), jnp.float32)
+    for j in range(4):
+        on = ids[:, j : j + 1] == lane
+        hit = hit + jnp.where(on, 1.0, 0.0)
+        gate = gate + jnp.where(on, gates[:, j : j + 1], 0.0)
+    hit_t = jnp.transpose(hit)
+    gate_t = jnp.transpose(gate)
+    before = (row < lane).astype(jnp.float32).astype(jnp.bfloat16)
+    rank_t = jnp.dot(hit_t.astype(jnp.bfloat16), before, preferred_element_type=jnp.float32)
+    key_t = jnp.where(hit_t > 0.0, rank_t, -1.0).astype(jnp.bfloat16)
+    gate_hi = gate_t.astype(jnp.bfloat16)
+    gate_lo = (gate_t - gate_hi.astype(jnp.float32)).astype(jnp.bfloat16)
+
+    loads[0].wait()
+    rows = rows_ref[...]
+    total = jnp.zeros((128, 1), jnp.float32)
+    for n in range(4):
+        cols = pl.ds(n * 512, 512)
+        part = jnp.dot(rows, w[:, cols], preferred_element_type=jnp.float32)
+        part = part + res_ref[:, cols].astype(jnp.float32)
+        mixed[:, cols] = part
+        total = total + jnp.sum(part * part, axis=1, keepdims=True)
+    scale = lax.rsqrt(total / 2048.0 + norm_eps)
+    normed[...] = (mixed[...] * scale * ngain_ref[...]).astype(jnp.bfloat16)
+
+    pl.semaphore_wait(barrier, N_DEV - 1)
+
+    def send_copy(k):
+        return pltpu.make_async_remote_copy(
+            src_ref=send.at[k, pl.ds(0, CAP)], dst_ref=recv.at[k, pl.ds(0, CAP)],
+            send_sem=s_sem, recv_sem=r_sem.at[k // PER],
+            device_id=shifted(me, k, 1), device_id_type=MESH)
+
+    def send_block(first, count, sem):
+        at = pl.ds(first, count)
+        return pltpu.make_async_remote_copy(
+            src_ref=send.at[at, pl.ds(0, CAP)], dst_ref=recv.at[at, pl.ds(0, CAP)],
+            send_sem=s_sem, recv_sem=sem, device_id=(sp, dp), device_id_type=MESH)
+
+    def pack(chunk, c):
+        step = chunk * 16 + row // SLOT
+        d = (step * 37) & 127
+        z = (me[0] + (d >> 5)) & 3
+        y = (me[1] + (d >> 3)) & 3
+        x = (me[2] + (d >> 1)) & 3
+        co = (me[3] + d) & 1
+        dest = z * 32 + y * 8 + x * 2 + co
+        rep = (dest == lane).astype(jnp.float32).astype(jnp.bfloat16)
+        key = jnp.dot(rep, key_t, preferred_element_type=jnp.float32)
+        on = key == (row & (SLOT - 1)).astype(jnp.float32)
+        pick = jnp.where(on, 1.0, 0.0).astype(jnp.bfloat16)
+        hi = jnp.dot(rep, gate_hi, preferred_element_type=jnp.float32)
+        lo = jnp.dot(rep, gate_lo, preferred_element_type=jnp.float32)
+        at = pl.ds(pl.multiple_of(chunk * 128, 128), 128)
+        g_hi[at, :] = jnp.where(on, hi, 0.0).astype(jnp.bfloat16)
+        g_lo[at, :] = jnp.where(on, lo, 0.0).astype(jnp.bfloat16)
+        packed = jnp.dot(pick, normed[...], preferred_element_type=jnp.float32).astype(jnp.bfloat16)
+        send[pl.ds(pl.multiple_of(chunk * 16, 16), 16)] = packed.reshape(16, SLOT, 2048)
+
+        def start(i, c):
+            send_copy((chunk - 1) * 16 + i).start()
+            return c
+
+        lax.fori_loop(jnp.where(chunk == 1, 1, 0), jnp.where(chunk == 0, 0, 16), start, 0)
+        return c
+
+    lax.fori_loop(0, 8, pack, 0)
+    lax.fori_loop(112, 128, lambda k, c: (send_copy(k).start(), c)[1], 0)
+    recv[0] = send[0]
+
+    for c in loads[1:4]:
+        c.wait()
+    xs = normed[...]
+    hidden = silu_mul(
+        jnp.dot(xs, sg[...], preferred_element_type=jnp.float32),
+        jnp.dot(xs, su[...], preferred_element_type=jnp.float32)).astype(jnp.bfloat16)
+    for n in range(4):
+        cols = pl.ds(n * 512, 512)
+        mixed[:, cols] = mixed[:, cols] + jnp.dot(hidden, sd[:, cols], preferred_element_type=jnp.float32)
+
+    for c in loads[4:]:
+        c.wait()
+
+    def back_copy(k):
+        return pltpu.make_async_remote_copy(
+            src_ref=fout.at[k, pl.ds(0, CAP)], dst_ref=ret.at[k, pl.ds(0, CAP)],
+            send_sem=s2_sem, recv_sem=r2_sem,
+            device_id=shifted(me, k, -1), device_id_type=MESH)
+
+    def expert(g, c):
+        first = g * PER
+        lo = jnp.where(g == 0, 1, 0)
+
+        @pl.when(g == 0)
+        def _():
+            send_block(1, PER - 1, r_sem.at[0]).wait_recv()
+
+        @pl.when(g > 0)
+        def _():
+            send_block(pl.multiple_of(first, PER), PER, r_sem.at[g]).wait_recv()
+
+        at = pl.ds(pl.multiple_of(first, PER), PER)
+        x = recv[at].reshape(PER * SLOT, 2048)
+        hid[...] = silu_mul(
+            jnp.dot(x, eg[...], preferred_element_type=jnp.float32),
+            jnp.dot(x, eu[...], preferred_element_type=jnp.float32)).astype(jnp.bfloat16)
+        h = hid[...]
+        for n in range(4):
+            cols = pl.ds(n * 512, 512)
+            o = jnp.dot(h, ed[:, cols], preferred_element_type=jnp.float32).astype(jnp.bfloat16)
+            fout[at, :, cols] = o.reshape(PER, SLOT, 512)
+
+        def reply(i, c):
+            back_copy(first + i).start()
+            return c
+
+        lax.fori_loop(lo, PER, reply, 0)
+        return c
+
+    lax.fori_loop(0, GROUPS, expert, 0)
+
+    def clear(i, c):
+        ret[pl.ds(pl.multiple_of(i * 16, 16), 16), pl.ds(CAP, SLOT - CAP)] = jnp.zeros((16, SLOT - CAP, 2048), jnp.bfloat16)
+        return c
+
+    lax.fori_loop(0, 8, clear, 0)
+    ret[0, pl.ds(0, CAP)] = fout[0, pl.ds(0, CAP)]
+
+    send_block(1, N_DEV - 1, r_sem.at[0]).wait_send()
+    others = pl.ds(1, N_DEV - 1)
+    back_all = pltpu.make_async_remote_copy(
+        src_ref=fout.at[others, pl.ds(0, CAP)], dst_ref=ret.at[others, pl.ds(0, CAP)],
+        send_sem=s2_sem, recv_sem=r2_sem, device_id=(sp, dp), device_id_type=MESH)
+    back_all.wait_send()
+    back_all.wait_recv()
+    dims = (((0,), (0,)), ((), ()))
+    for n in range(4):
+        cols = pl.ds(n * 512, 512)
+        r = ret[:, :, cols].reshape(N_DEV * SLOT, 512)
+        routed = lax.dot_general(g_hi[...], r, dims, preferred_element_type=jnp.float32)
+        routed = routed + lax.dot_general(g_lo[...], r, dims, preferred_element_type=jnp.float32)
+        out_ref[:, cols] = (mixed[:, cols] + routed).astype(jnp.bfloat16)
+
+
+def moe(rows, w, res, ngain, ids, rw, sg, su, sd, eg, eu, ed):
+    bf, f32 = jnp.bfloat16, jnp.float32
+    V, A = pl.BlockSpec(memory_space=pltpu.VMEM), pl.BlockSpec(memory_space=pl.ANY)
+    S = pltpu.SemaphoreType.DMA
+    return pl.pallas_call(
+        moe_kernel,
+        out_shape=jax.ShapeDtypeStruct((128, 2048), bf),
+        in_specs=[V, A, V, V, V, V, A, A, A, A, A, A],
+        out_specs=V,
+        scratch_shapes=[
+            pltpu.VMEM((2048, 2048), bf),
+            pltpu.VMEM((2048, 512), bf), pltpu.VMEM((2048, 512), bf), pltpu.VMEM((512, 2048), bf),
+            pltpu.VMEM((2048, 512), bf), pltpu.VMEM((2048, 512), bf), pltpu.VMEM((512, 2048), bf),
+            pltpu.VMEM((128, 2048), f32), pltpu.VMEM((128, 2048), bf),
+            pltpu.VMEM((1024, 128), bf), pltpu.VMEM((1024, 128), bf),
+            pltpu.VMEM((128, SLOT, 2048), bf), pltpu.VMEM((128, SLOT, 2048), bf),
+            pltpu.VMEM((128, SLOT, 2048), bf), pltpu.VMEM((128, SLOT, 2048), bf),
+            pltpu.VMEM((PER * SLOT, 512), bf),
+            S((7,)), S, S((GROUPS,)), S, S,
+        ],
+        compiler_params=pltpu.CompilerParams(collective_id=0, has_side_effects=True, vmem_limit_bytes=62 * 2**20),
+        name="moe",
+    )(rows, w, res, ngain, ids, rw, sg, su, sd, eg, eu, ed)
 
 
 def rotate_half(values, position, half_width):
@@ -114,54 +339,11 @@
         tiled=True,
     )
     flat_rows = returned_heads.reshape(tokens, -1)
-    projected = jnp.dot(
-        flat_rows,
-        lax.all_gather(out_weight, "dp", axis=1, tiled=True),
-        preferred_element_type=jnp.float32,
-    )
-    mixed = residual[0].astype(jnp.float32) + projected
-    normed = mixed * lax.rsqrt(jnp.mean(mixed * mixed, axis=-1, keepdims=True) + norm_eps)
-    normed = (normed * norm_gain).astype(jnp.bfloat16)
-    shared = swiglu(normed, shared_gate, shared_up, shared_down)
-    local_experts = expert_gate.shape[0]
-    experts = local_experts * lax.axis_size(("sp", "dp"))
-    top_count = route_ids.shape[2]
-    slot_count = max(2, 3 * tokens * top_count // (2 * experts))
-    route_list = route_ids[0].reshape(-1)
-    raw_weights = route_weights[0]
-    gate_values = (
-        raw_weights / jnp.sum(raw_weights, axis=-1, keepdims=True) * routed_scale
-    ).reshape(-1)
-    hit_table = (route_list[:, None] == jnp.arange(experts, dtype=jnp.int32)[None, :]).astype(
-        jnp.int32
-    )
-    slot_rank = jnp.sum((jnp.cumsum(hit_table, axis=0) - hit_table) * hit_table, axis=1)
-    slot_place = route_list * slot_count + slot_rank
-    outgoing = jnp.zeros((experts * slot_count, model_width), jnp.bfloat16)
-    outgoing = outgoing.at[slot_place].set(jnp.repeat(normed, top_count, axis=0))
-    outgoing = outgoing.reshape(experts, slot_count, model_width)
-    arrived = lax.all_to_all(outgoing, ("sp", "dp"), split_axis=0, concat_axis=0, tiled=True)
-    sources = arrived.shape[0] // local_experts
-    slot_width = arrived.shape[1]
-    grouped = arrived.reshape(sources, local_experts, slot_width, model_width)
-    row_block = grouped[:, 0].reshape(-1, model_width)
-    output = swiglu(row_block, expert_gate[0], expert_up[0], expert_down[0])
-    results = [output.astype(jnp.bfloat16).reshape(sources, slot_width, model_width)]
-    returned = lax.all_to_all(
-        jnp.stack(results, axis=1).reshape(arrived.shape),
-        ("sp", "dp"),
-        split_axis=0,
-        concat_axis=0,
-        tiled=True,
-    )
-    gathered = returned.reshape(experts * slot_count, model_width)[slot_place]
-    routed = jnp.sum(
-        (gathered.astype(jnp.float32) * gate_values[:, None]).reshape(
-            tokens, top_count, model_width
-        ),
-        axis=1,
-    )
-    combined = (mixed + shared + routed).astype(jnp.bfloat16)
+    full_weight = lax.all_gather(out_weight, "dp", axis=1, tiled=True)
+    combined = moe(
+        flat_rows, full_weight, residual[0], norm_gain[None, :], route_ids[0], route_weights[0],
+        shared_gate, shared_up, shared_down, expert_gate, expert_up, expert_down,
+    )
     return combined.reshape(1, tokens, model_width)
 
 

time: 319 us -> 197 us (0.62)
  Pallas kernels: 0 us -> 89.1 us
  local copies, waits for them, and re-layouts: 78.9 us -> 15.4 us
  blocking collectives: 62.2 us -> 0 us
  waiting for transfers between devices: 67.6 us -> 19.5 us
  matrix products: 37.2 us -> 14.8 us
  other arithmetic: 35 us -> 27.1 us
  starting transfers between devices: 22.7 us -> 15.7 us
    pallas_call x0 -> x1, Pallas kernels: none -> 89.1 us  [moe(): pl.pallas_call(moe_kernel, out_shape=jax.ShapeDtypeStruct((128, 2048), bf...]
    all_to_all x1 -> x0, blocking collectives: 62.2 us -> none  [per_device(): lax.all_to_all(outgoing, ('sp', 'dp'), split_axis=0, concat_axis=0, tiled...]
    all_to_all x1 -> x0, waiting for transfers between devices: 50.3 us -> none  [per_device(): lax.all_to_all(jnp.stack(results, axis=1).reshape(arrived.shape), ('sp',...]
    dot_general x5 -> x0, matrix products: 25.1 us -> none  [the longest x2 12.5 us: swiglu(): return jnp.dot(hidden, down_weight, preferred_element_type=jnp.float32)]
    reshape x3 -> x0, local copies, waits for them, and re-layouts: 16.5 us -> none  [the longest x1 6.32 us: per_device(): gathered = returned.reshape(experts * slot_count, model_width)[slot_place]]
    another operation x5 -> x0, local copies, waits for them, and re-layouts: 13.3 us -> none  [the longest x1 6.31 us: per_device(): row_block = grouped[:, 0].reshape(-1, model_width)]
    gather x1 -> x0, local copies, waits for them, and re-layouts: 7.58 us -> none  [per_device(): gathered = returned.reshape(experts * slot_count, model_width)[slot_place]]
    scatter x1 -> x0, local copies, waits for them, and re-layouts: 6.72 us -> none  [per_device(): outgoing.at[slot_place].set(jnp.repeat(normed, top_count, axis=0))]
  transfers between devices with their start and end apart: 5 -> 4, of which waited for: 4 -> 3; matrix products, arithmetic and copies ran while one was open for 22% -> 28% of each run, Pallas kernels for 0% -> 0%
where the time goes in v1:
time: 197 us; the launch traced here: 195 us
  Pallas kernels  89.1 us (45%)
  other arithmetic  27.1 us (14%)
  waiting for transfers between devices  19.5 us (10%)
  starting transfers between devices  15.7 us (8%)
  local copies, waits for them, and re-layouts  15.4 us (8%)
  matrix products  14.8 us (8%)
  between operations  13.7 us (7%)
    pallas_call x1, Pallas kernels, moe(): pl.pallas_call(moe_kernel, out_shape=jax.ShapeDtypeStruct((128, 2048), bf...  89.1 us
    unnamed x1, other arithmetic  11.7 us
    unnamed x20, local copies, waits for them, and re-layouts  10.7 us
    dot_general x4, matrix products, one_block(): jnp.einsum('grqk,kgd->grqd', rounded, values, preferred_element_type=jnp....  9.28 us
    all_to_all x1, starting transfers between devices, per_device(): lax.all_to_all(query, 'sp', split_axis=2, concat_axis=1, tiled=True)  8.59 us
    all_to_all x1, waiting for transfers between devices, per_device(): lax.all_to_all(attention.reshape(1, length, kv_local, repeats * head_dim)...  7.48 us
    reduce_sum x4, other arithmetic, one_block(): row_total = jnp.sum(weights, axis=-1, keepdims=True)  6.55 us
    all_to_all x1, waiting for transfers between devices, per_device(): lax.all_to_all(key_value, 'sp', split_axis=2, concat_axis=1, tiled=True)  6.31 us
  transfers between devices with their start and end apart: 4, of which 3 were waited for; matrix products, arithmetic and copies ran while one was open for 28% of the time, Pallas kernels for 0%

profile of v1, /device:TPU:1, one launch (start us, length us, event | category | flops | bytes accessed | tf_op | source)
XLA Modules:
  0.0 195.2 jit_solution(13845488617417471296)
XLA Ops:
  7.3 2.0 %copy.31 = bf16[1,128,16,128]{3,1,0,2:T(8,128)(2,1)} copy(bf16[1,128,16,128]{3,2,1,0:T(8,128)(2,1)} %param.18) | data formatting | bytes 1048576 | tf_op args[1]
  9.3 8.6 %all-to-all-start = ((bf16[1,128,16,128]{3,1,0,2:T(8,128)(2,1)}), bf16[1,128,16,128]{3,1,0,2:T(8,128)(2,1)S(1)}, u32[]{:S(2)}, u32[]{:S(2)}) async-start(bf16[1,128,16,128]{3,1,0,2:T(8,128)(2,1)} %copy.31), calls=%async_computation | async-start | bytes 1048576 | tf_op jit(solution)/shard_map/all_to_all | solution.py:318
  17.9 2.0 %copy.33 = bf16[1,128,16,128]{3,1,0,2:T(8,128)(2,1)} copy(bf16[1,128,16,128]{3,2,1,0:T(8,128)(2,1)} %param.19) | data formatting | bytes 1048576 | tf_op args[2]
  19.9 0.8 fusion.45
  20.7 2.6 %fusion.36 = (f32[2048,32]{0,1:T(8,128)S(1)}, f32[2048,32]{0,1:T(8,128)S(1)}, f32[2048,32]{0,1:T(8,128)S(1)}, f32[2048,32]{0,1:T(8,128)}) fusion(f32[2048,16]{0,1:T(8,128)S(1)} %get-tuple-element.74, f32[2048,16]{0,1:T(8,128)S(1)} %get-tuple-element.77), kind=kLoop, calls=%fused_computation.45 | loop fusion | flops 131072 | bytes 1310720 | tf_op jit(solution)/shard_map/cos | solution.py:243
  23.3 5.0 %all-to-all-done = bf16[1,128,16,128]{3,1,0,2:T(8,128)(2,1)S(1)} async-done(((bf16[1,128,16,128]{3,1,0,2:T(8,128)(2,1)}), bf16[1,128,16,128]{3,1,0,2:T(8,128)(2,1)S(1)}, u32[]{:S(2)}, u32[]{:S(2)}) %all-to-all-start) | async-done | bytes 524320 | tf_op jit(solution)/shard_map/all_to_all | solution.py:318
  28.3 3.6 %all-to-all-start.1 = ((bf16[1,128,16,128]{3,1,0,2:T(8,128)(2,1)}), bf16[1,128,16,128]{3,1,0,2:T(8,128)(2,1)S(1)}, u32[]{:S(2)}, u32[]{:S(2)}) async-start(bf16[1,128,16,128]{3,1,0,2:T(8,128)(2,1)} %copy.33), calls=%async_computation.1 | async-start | bytes 1048576 | tf_op jit(solution)/shard_map/all_to_all | solution.py:319
  33.1 1.2 fusion.30
  35.1 6.3 %all-to-all-done.1 = bf16[1,128,16,128]{3,1,0,2:T(8,128)(2,1)S(1)} async-done(((bf16[1,128,16,128]{3,1,0,2:T(8,128)(2,1)}), bf16[1,128,16,128]{3,1,0,2:T(8,128)(2,1)S(1)}, u32[]{:S(2)}, u32[]{:S(2)}) %all-to-all-start.1) | async-done | bytes 524320 | tf_op jit(solution)/shard_map/all_to_all | solution.py:319
  42.3 3.1 %fusion.34 = (bf16[2048,1,32]{0,2,1:T(8,128)(2,1)S(1)}, bf16[2048,1,32]{0,2,1:T(8,128)(2,1)S(1)}) fusion(f32[2048,1,64]{0,2,1:T(8,128)S(1)} %fusion.26, f32[2048,1,16]{0,2,1:T(8,128)S(1)} %get-tuple-element.73, f32[2048,1,16]{0,2,1:T(8,128)S(1)} %get-tuple-element.68, f32[2048,1,16]{0,2,1:T(8,128)S(1)} %get-tuple-element.65, ...), kind=kLoop, calls=%fused_computation.40 | loop fusion | flops 786432 | bytes 1572864 | tf_op jit(solution)/shard_map/convert.3
  45.5 21.3 %while.10 = (s32[]{:T(128)}, bf16[4,512,1,2,64]{1,4,3,2,0:T(8,128)(2,1)}, bf16[4,512,1,2,64]{1,4,3,2,0:T(8,128)(2,1)S(1)}, bf16[2048,1,64]{0,2,1:T(8,128)(2,1)S(1)}, bf16[2048,1,64]{0,2,1:T(8,128)(2,1)S(1)}, /*index=5*/s32[]{:T(128)}) while((s32[]{:T(128)}, bf16[4,512,1,2,64]{1,4,3,2,0:T(8,128)(2,1)}, ...), condition=%wide.region_5.6_spmd, body=%wide.region_2.5_spmd.sunk | while | flops 553777152 | bytes 25973320 | solution.py:287
  45.5 1.4 bitcast_reduce_fusion.2
  46.9 1.6 fusion.63
  48.5 2.3 %fusion.64 = bf16[4,512,1,2,64]{1,4,3,2,0:T(8,128)(2,1)} fusion(bf16[4,512,1,2,64]{1,4,3,2,0:T(8,128)(2,1)} %get-tuple-element.123, s32[]{:T(128)} %get-tuple-element.122, f32[512,2,2048]{2,0,1:T(8,128)S(1)} %get-tuple-element.114, f32[2,512]{1,0:T(2,128)S(1)} %get-tuple-element.115, bf16[2048,1,64]{0,2,1:T(8,128)(2,1)S(1)} %get-tuple-element.132, ...), kind=kOutput, calls=%fused_computation.10.clone.1 | convolution fusion | flops 274857984 | bytes 8790528 | tf_op jit(solution)/shard_map/while/body/eval_jaxpr/grqk,kgd->grqd/dot_general | solution.py:281
  50.9 1.4 bitcast_reduce_fusion.2
  52.2 1.6 fusion.63
  53.9 2.3 %fusion.64 = bf16[4,512,1,2,64]{1,4,3,2,0:T(8,128)(2,1)} fusion(bf16[4,512,1,2,64]{1,4,3,2,0:T(8,128)(2,1)} %get-tuple-element.123, s32[]{:T(128)} %get-tuple-element.122, f32[512,2,2048]{2,0,1:T(8,128)S(1)} %get-tuple-element.114, f32[2,512]{1,0:T(2,128)S(1)} %get-tuple-element.115, bf16[2048,1,64]{0,2,1:T(8,128)(2,1)S(1)} %get-tuple-element.132, ...), kind=kOutput, calls=%fused_computation.10.clone.1 | convolution fusion | flops 274857984 | bytes 8790528 | tf_op jit(solution)/shard_map/while/body/eval_jaxpr/grqk,kgd->grqd/dot_general | solution.py:281
  56.2 1.4 bitcast_reduce_fusion.2
  57.6 1.6 fusion.63
  59.2 2.3 %fusion.64 = bf16[4,512,1,2,64]{1,4,3,2,0:T(8,128)(2,1)} fusion(bf16[4,512,1,2,64]{1,4,3,2,0:T(8,128)(2,1)} %get-tuple-element.123, s32[]{:T(128)} %get-tuple-element.122, f32[512,2,2048]{2,0,1:T(8,128)S(1)} %get-tuple-element.114, f32[2,512]{1,0:T(2,128)S(1)} %get-tuple-element.115, bf16[2048,1,64]{0,2,1:T(8,128)(2,1)S(1)} %get-tuple-element.132, ...), kind=kOutput, calls=%fused_computation.10.clone.1 | convolution fusion | flops 274857984 | bytes 8790528 | tf_op jit(solution)/shard_map/while/body/eval_jaxpr/grqk,kgd->grqd/dot_general | solution.py:281
  61.5 1.4 bitcast_reduce_fusion.2
  62.9 1.6 fusion.63
  64.5 2.3 %fusion.64 = bf16[4,512,1,2,64]{1,4,3,2,0:T(8,128)(2,1)} fusion(bf16[4,512,1,2,64]{1,4,3,2,0:T(8,128)(2,1)} %get-tuple-element.123, s32[]{:T(128)} %get-tuple-element.122, f32[512,2,2048]{2,0,1:T(8,128)S(1)} %get-tuple-element.114, f32[2,512]{1,0:T(2,128)S(1)} %get-tuple-element.115, bf16[2048,1,64]{0,2,1:T(8,128)(2,1)S(1)} %get-tuple-element.132, ...), kind=kOutput, calls=%fused_computation.10.clone.1 | convolution fusion | flops 274857984 | bytes 8790528 | tf_op jit(solution)/shard_map/while/body/eval_jaxpr/grqk,kgd->grqd/dot_general | solution.py:281
  66.9 2.3 %copy.42 = bf16[4,512,1,2,64]{4,3,1,0,2:T(2,128)(2,1)S(1)} copy(bf16[4,512,1,2,64]{1,4,3,2,0:T(8,128)(2,1)} %get-tuple-element.32) | data formatting | bytes 1048576 | tf_op jit(solution)/shard_map/reshape;reshape | solution.py:335
  70.4 11.7 %reduce.3 = bf16[2048,128]{1,0:T(8,128)(2,1)S(1)} reduce(bf16[2048,1,1,128]{3,2,1,0:T(2,128)(2,1)S(1)} %bitcast.116, bf16[]{:T(256)} %broadcast.238), dimensions={1,2}, to_apply=%bitcast.91.reduce_sub_computation | reduce | bytes 1048578
  82.1 0.9 reshape.480
  83.0 3.6 %all-to-all-start.2 = ((bf16[16,2,8192]{2,1,0:T(2,128)(2,1)}), bf16[16,2,8192]{2,1,0:T(2,128)(2,1)S(1)}, u32[]{:S(2)}, u32[]{:S(2)}) async-start(bf16[16,2,8192]{2,1,0:T(2,128)(2,1)} %reshape.480), calls=%async_computation.2 | async-start | bytes 1048576 | tf_op jit(solution)/shard_map/all_to_all | solution.py:334
  86.6 0.7 copy.40
  88.1 7.5 %all-to-all-done.2 = bf16[16,2,8192]{2,1,0:T(2,128)(2,1)S(1)} async-done(((bf16[16,2,8192]{2,1,0:T(2,128)(2,1)}), bf16[16,2,8192]{2,1,0:T(2,128)(2,1)S(1)}, u32[]{:S(2)}, u32[]{:S(2)}) %all-to-all-start.2) | async-done | bytes 524320 | tf_op jit(solution)/shard_map/all_to_all | solution.py:334
  96.5 0.9 copy.49
  97.4 89.1 %moe.1 = bf16[128,2048]{1,0:T(8,128)(2,1)} custom-call(bf16[128,2048]{1,0:T(8,128)(2,1)} %bitcast.117, bf16[2048,2048]{1,0:T(8,128)(2,1)} %all-gather.2.cloned.1.call-done.w_ref, bf16[128,2048]{1,0:T(8,128)(2,1)} %bitcast.121, f32[1,2048]{1,0:T(1,128)} %bitcast.124, s32[128,4]{1,0:T(8,128)} %bitcast.122, f32[128,4]{1,0:T(8,128)} %bitcast.123, ...), custom_call_target="tpu_custom_call" | custom-call | tf_op jit(solution)/shard_map/moe/pallas_call | solution.py:218
  186.5 1.9 copy.60
  (40 shorter events, 6.4 us)
Async XLA Ops:
  6.5 26.3 %copy-start.2 = (f32[64]{0:T(128)S(1)}, f32[64]{0:T(128)}, u32[]{:S(2)}) copy-start(f32[64]{0:T(128)} %param.22) | copy-start | bytes 772
  6.5 90.9 %all-gather.2.cloned.1.call-start = ((), (), s32[]{:S(2)}) async-start(), calls=%async_computation.3 | async-start | bytes 9437184 | tf_op jit(solution)/shard_map/all_gather | solution.py:342
  9.3 19.0 %all-to-all-start = ((bf16[1,128,16,128]{3,1,0,2:T(8,128)(2,1)}), bf16[1,128,16,128]{3,1,0,2:T(8,128)(2,1)S(1)}, u32[]{:S(2)}, u32[]{:S(2)}) async-start(bf16[1,128,16,128]{3,1,0,2:T(8,128)(2,1)} %copy.31), calls=%async_computation | async-start | bytes 1048576 | tf_op jit(solution)/shard_map/all_to_all | solution.py:318
  28.3 13.2 %all-to-all-start.1 = ((bf16[1,128,16,128]{3,1,0,2:T(8,128)(2,1)}), bf16[1,128,16,128]{3,1,0,2:T(8,128)(2,1)S(1)}, u32[]{:S(2)}, u32[]{:S(2)}) async-start(bf16[1,128,16,128]{3,1,0,2:T(8,128)(2,1)} %copy.33), calls=%async_computation.1 | async-start | bytes 1048576 | tf_op jit(solution)/shard_map/all_to_all | solution.py:319
  32.7 9.5 %copy-start.3 = (f32[64]{0:T(128)S(1)}, f32[64]{0:T(128)}, u32[]{:S(2)}) copy-start(f32[64]{0:T(128)} %param.23) | copy-start | bytes 772
  45.5 41.1 %copy-start = (s32[1,128,4]{1,2,0:T(4,128)S(1)}, s32[1,128,4]{1,2,0:T(4,128)}, u32[]{:S(2)}) copy-start(s32[1,128,4]{1,2,0:T(4,128)} %param.24) | copy-start | bytes 6148
  45.5 41.8 %copy-start.1 = (f32[1,128,4]{1,2,0:T(4,128)S(1)}, f32[1,128,4]{1,2,0:T(4,128)}, u32[]{:S(2)}) copy-start(f32[1,128,4]{1,2,0:T(4,128)} %param.25) | copy-start | bytes 6148
  83.0 12.5 %all-to-all-start.2 = ((bf16[16,2,8192]{2,1,0:T(2,128)(2,1)}), bf16[16,2,8192]{2,1,0:T(2,128)(2,1)S(1)}, u32[]{:S(2)}, u32[]{:S(2)}) async-start(bf16[16,2,8192]{2,1,0:T(2,128)(2,1)} %reshape.480), calls=%async_computation.2 | async-start | bytes 1048576 | tf_op jit(solution)/shard_map/all_to_all | solution.py:334
Sparse Core Ops, SparseCore 0:
  9.0 56.9 all-gather.1

commit v2 on v1

v2 whole, which is shorter than its diff:
```python
import math
import jax
import jax.numpy as jnp
from jax import lax
from jax.experimental import pallas as pl
from jax.experimental.pallas import tpu as pltpu
import numpy as np
from jax.sharding import PartitionSpec as P

MESH = pl.DeviceIdType.MESH
N_DEV = 128
CAP = 6
SLOT = 8
GROUPS = 4
PER = N_DEV // GROUPS
norm_eps = 1e-06
rope_theta = 10000.0
routed_scale = 2.5
N_SP = 16
LEN = 2048
BLOCKS = 8
EXP_SCALE = 0.125 * math.log2(math.e)


def digits(n):
    return n // 32, (n // 8) % 4, (n // 2) % 4, n % 2


def shifted(me_digits, k, sign):
    d = lax.rem(k * 37, 128)
    out = []
    for m, v, size in zip(me_digits, digits(d), (4, 4, 4, 2)):
        out.append(lax.rem(m + sign * v + size, size))
    z, y, x, c = out
    return z * 4 + y, x * 2 + c


def silu_mul(g, u):
    return g / (1.0 + jnp.exp(-g)) * u


def sp_shifted(me, k, sign):
    d = lax.rem(k * 7, 16)
    z = lax.rem(me[0] + sign * (d // 4) + 4, 4)
    y = lax.rem(me[1] + sign * lax.rem(d, 4) + 4, 4)
    return z * 4 + y


def rope_tables():
    lanes = np.arange(128)
    theta = (np.float32(rope_theta) ** (-(2 * (lanes % 16)).astype(np.float32) / np.float32(32))).astype(np.float32)
    angles = np.arange(64, dtype=np.float32)[:, None] * theta[None, :]
    sign = np.where(lanes % 32 < 16, -1.0, 1.0)
    return np.cos(angles).astype(np.float32), (np.sin(angles) * sign).astype(np.float32)


def layer_kernel(
    q_ref, kv_ref, cos_ref, sin_ref, qg_ref, kg_ref,
    w_ref, res_ref, ngain_ref, ids_ref, rw_ref, sg_ref, su_ref, sd_ref, eg_ref, eu_ref, ed_ref,
    out_ref,
    w, sg, su, sd, eg, eu, ed, mixed, normed, g_hi, g_lo, send, recv, fout, ret, hid,
    wide, sq, skv, rq, rkv, kt, vx, ao, rows,
    ld_sem, s_sem, r_sem, s2_sem, r2_sem, kvs_sem, kvr_sem, qs_sem, qr_sem, bs_sem, br_sem, ws_sem, wr_sem,
):
    sp = lax.axis_index("sp")
    dp = lax.axis_index("dp")
    me = (sp // 4, lax.rem(sp, 4), dp // 2, lax.rem(dp, 2))

    own_cols = pl.ds(pl.multiple_of(dp * 256, 256), 256)
    loads = [
        pltpu.make_async_copy(a, b, ld_sem.at[i])
        for i, (a, b) in enumerate(
            [(w_ref, w.at[:, own_cols]), (sg_ref, sg), (su_ref, su), (sd_ref, sd), (eg_ref.at[0], eg), (eu_ref.at[0], eu), (ed_ref.at[0], ed)]
        )
    ]
    for c in loads:
        c.start()
    barrier = pltpu.get_barrier_semaphore()

    def greet(k, c):
        pl.semaphore_signal(barrier, inc=1, device_id=shifted(me, k, 1), device_id_type=MESH)
        return c

    lax.fori_loop(1, N_DEV, greet, 0)

    lane = lax.broadcasted_iota(jnp.int32, (128, 128), 1)
    row = lax.broadcasted_iota(jnp.int32, (128, 128), 0)

    lane1 = lax.broadcasted_iota(jnp.int32, (1, 128), 1)
    swap_up = (lane1 & 31) < 16

    def turned_gain(g):
        return jnp.where(swap_up, pltpu.roll(g, 112, 1), pltpu.roll(g, 16, 1))

    def both(g):
        return jnp.concatenate([g, g], axis=1)

    col_lane = (lane1 & 63) >= 32
    first = pl.ds(0, 64)
    second = pl.ds(64, 64)
    q_gain, k_gain = both(qg_ref[...]), both(kg_ref[...])
    q_gain8, k_gain8 = jnp.broadcast_to(q_gain, (8, 128)), jnp.broadcast_to(k_gain, (8, 128))
    q_turn, k_turn = turned_gain(q_gain8)[0:1], turned_gain(k_gain8)[0:1]

    def table(ref):
        top = jnp.where(col_lane, ref[...], ref[pl.ds(sp * 2, 1), :])
        bottom = jnp.where(col_lane, ref[...], ref[pl.ds(sp * 2 + 1, 1), :])
        return jnp.concatenate([top, bottom], axis=0)

    cosine, sine = table(cos_ref), table(sin_ref)
    ones_block = ((row >> 6) == (lane >> 6)).astype(jnp.float32).astype(jnp.bfloat16)
    turn = ((row ^ 16) == lane).astype(jnp.float32).astype(jnp.bfloat16)

    def prepared(x, cos_gain, sin_gain):
        xb = x.astype(jnp.bfloat16)
        square = x * x
        high = square.astype(jnp.bfloat16)
        low = (square - high.astype(jnp.float32)).astype(jnp.bfloat16)
        total = jnp.dot(high, ones_block, preferred_element_type=jnp.float32)
        total = total + jnp.dot(low, ones_block, preferred_element_type=jnp.float32)
        other = jnp.dot(xb, turn, preferred_element_type=jnp.float32)
        return lax.rsqrt(total / 64.0 + norm_eps) * (x * cos_gain + other * sin_gain)

    def prepare_all(source, target, cos_gain, sin_gain, keep):
        wide[...] = source[...].astype(jnp.float32).reshape(LEN, 128)

        def one(k, c):
            x = wide[pl.ds(sp_shifted(me, k, 1), 128, stride=16), :]
            y = prepared(x, cos_gain, sin_gain)
            if keep:
                y = jnp.where(lane < 64, y, x)
            target[k] = y.astype(jnp.bfloat16)
            return c

        lax.fori_loop(0, N_SP, one, 0)

    prepare_all(kv_ref, skv, cosine * k_gain, sine * k_turn, True)
    prepare_all(q_ref, sq, cosine * q_gain, sine * q_turn, False)

    pl.semaphore_wait(barrier, N_DEV - 1)

    def sp_copy(src, dst, k, sign, s, r):
        return pltpu.make_async_remote_copy(
            src_ref=src, dst_ref=dst, send_sem=s, recv_sem=r,
            device_id=(sp_shifted(me, k, sign), dp), device_id_type=MESH)

    def send_kv(k, c):
        sp_copy(skv.at[k], rkv.at[k], k, 1, kvs_sem, kvr_sem).start()
        return c

    def send_q(k, c):
        sp_copy(sq.at[k], rq.at[k], k, 1, qs_sem, qr_sem.at[k // 2]).start()
        return c

    lax.fori_loop(1, N_SP, send_kv, 0)
    lax.fori_loop(1, N_SP, send_q, 0)

    loads[0].wait()
    x_at, core = me[2], me[3]
    right, left = lax.rem(x_at + 1, 4), lax.rem(x_at + 3, 4)

    def w_copy(x_from, core_from, half, x_to, core_to, number):
        size = LEN if half is None else LEN // 2
        at = w.at[pl.ds(0 if half is None else half * size, size), pl.ds(pl.multiple_of((x_from * 2 + core_from) * 256, 256), 256)]
        return pltpu.make_async_remote_copy(
            src_ref=at, dst_ref=at, send_sem=ws_sem, recv_sem=wr_sem.at[number],
            device_id=(sp, x_to * 2 + core_to), device_id_type=MESH)

    w_copy(x_at, core, 0, right, core, 0).start()
    w_copy(x_at, core, 1, left, core, 1).start()
    w_copy(x_at, core, 1, right, core, 2).start()
    w_copy(x_at, core, 0, left, core, 3).start()
    w_copy(x_at, core, None, x_at, 1 - core, 4).start()
    far = lax.rem(x_at + 2, 4)
    early = ((left, 0, 0), (right, 1, 1))
    later = ((left, 1, 2), (right, 0, 3))
    last = ((far, 0, 5), (far, 1, 6))

    def w_relay():
        for x_from, half, number in early:
            w_copy(x_from, core, half, right, core, number).wait_recv()
        w_copy(left, core, 0, right, core, 5).start()
        w_copy(right, core, 1, left, core, 6).start()
        for x_from, half, number in early:
            w_copy(x_from, core, half, x_at, 1 - core, 7 + number).start()

    def w_share(some):
        for x_from, half, number in some:
            w_copy(x_from, core, half, right, core, number).wait_recv()
            w_copy(x_from, core, half, x_at, 1 - core, 7 + number).start()

    def w_finish():
        w_copy(x_at, 1 - core, None, x_at, core, 4).wait_recv()
        for x_from, half, number in early + later + last:
            w_copy(x_from, 1 - core, half, x_at, core, 7 + number).wait_recv()
        everything = w.at[:, pl.ds(0, 7 * 256)]
        pltpu.make_async_remote_copy(
            src_ref=everything, dst_ref=everything, send_sem=ws_sem, recv_sem=wr_sem.at[0],
            device_id=(sp, dp), device_id_type=MESH).wait_send()

    raw = rw_ref[...]
    gates = raw / jnp.sum(raw, axis=1, keepdims=True) * routed_scale
    ids = ids_ref[...]
    hit = jnp.zeros((128, 128), jnp.float32)
    gate = jnp.zeros((128, 128), jnp.float32)
    for j in range(4):
        on = ids[:, j : j + 1] == lane
        hit = hit + jnp.where(on, 1.0, 0.0)
        gate = gate + jnp.where(on, gates[:, j : j + 1], 0.0)
    hit_t = jnp.transpose(hit)
    gate_t = jnp.transpose(gate)
    before = (row < lane).astype(jnp.float32).astype(jnp.bfloat16)
    rank_t = jnp.dot(hit_t.astype(jnp.bfloat16), before, preferred_element_type=jnp.float32)
    key_t = jnp.where(hit_t > 0.0, rank_t, -1.0).astype(jnp.bfloat16)
    gate_hi = gate_t.astype(jnp.bfloat16)
    gate_lo = (gate_t - gate_hi.astype(jnp.float32)).astype(jnp.bfloat16)

    def clear(i, c):
        ret[pl.ds(pl.multiple_of(i * 16, 16), 16), pl.ds(CAP, SLOT - CAP)] = jnp.zeros((16, SLOT - CAP, 2048), jnp.bfloat16)
        return c

    lax.fori_loop(0, 8, clear, 0)

    rkv[0] = skv[0]
    rq[0] = sq[0]
    others16 = pl.ds(1, N_SP - 1)

    def sp_all(src, dst, s, r):
        return pltpu.make_async_remote_copy(
            src_ref=src, dst_ref=dst, send_sem=s, recv_sem=r, device_id=(sp, dp), device_id_type=MESH)

    sp_all(skv.at[others16], rkv.at[others16], kvs_sem, kvr_sem).wait_recv()

    def lay(k, c):
        pair = rkv[k].astype(jnp.float32)
        swapped = pltpu.roll(pair, 64, 1)
        low_lane = lane < 64
        at = pl.ds(pl.multiple_of(k * 128, 128), 128)
        at2 = pl.ds(pl.multiple_of(LEN + k * 128, 128), 128)
        kt[:, at] = jnp.transpose(jnp.where(low_lane, pair, 0.0)).astype(jnp.bfloat16)
        kt[:, at2] = jnp.transpose(jnp.where(low_lane, 0.0, swapped)).astype(jnp.bfloat16)
        vx[at, pl.ds(0, 128)] = jnp.where(low_lane, swapped, 0.0).astype(jnp.bfloat16)
        vx[at2, pl.ds(0, 128)] = jnp.where(low_lane, 0.0, pair).astype(jnp.bfloat16)
        vx[at, pl.ds(128, 128)] = jnp.where(low_lane, 1.0, 0.0).astype(jnp.bfloat16)
        vx[at2, pl.ds(128, 128)] = jnp.where(low_lane, 0.0, 1.0).astype(jnp.bfloat16)
        return c

    lax.fori_loop(0, N_SP, lay, 0)
    own_rows = pl.ds(pl.multiple_of(sp * 128, 128), 128)

    def back_rows(k):
        return sp_copy(ao.at[k], rows.at[:, own_rows], k, -1, bs_sem, br_sem)

    def block(b, c):
        @pl.when(b == 0)
        def _():
            sp_all(sq.at[1], rq.at[1], qs_sem, qr_sem.at[0]).wait_recv()

        @pl.when(b > 0)
        def _():
            two = pl.ds(b * 2, 2)
            sp_all(sq.at[two], rq.at[two], qs_sem, qr_sem.at[b]).wait_recv()

        q = rq[pl.ds(b * 2, 2)].reshape(256, 128)
        o = jnp.zeros((256, 256), jnp.float32)
        for h in range(2):
            keys = pl.ds(h * LEN, LEN)
            s = jnp.dot(q, kt[:, keys], preferred_element_type=jnp.float32)
            top = jnp.max(s, axis=1, keepdims=True)
            p = jnp.exp2((s - top) * EXP_SCALE).astype(jnp.bfloat16)
            o = o + jnp.dot(p, vx[keys, :], preferred_element_type=jnp.float32)
        a = (o[:, :128] / o[:, 128:]).astype(jnp.bfloat16)
        ao[pl.ds(b * 2, 2)] = a.reshape(2, 128, 128)

        @pl.when(b > 0)
        def _():
            back_rows(b * 2).start()

        back_rows(b * 2 + 1).start()

        @pl.when(b == 4)
        def _():
            w_relay()

        return c

    lax.fori_loop(0, BLOCKS, block, 0)
    rows[:, own_rows] = ao[0]
    sp_all(skv.at[others16], rkv.at[others16], kvs_sem, kvr_sem).wait_send()
    sp_all(sq.at[others16], rq.at[others16], qs_sem, qr_sem.at[0]).wait_send()
    w_share(later)
    w_share(last)
    w_finish()
    back_all16 = sp_all(ao.at[others16], ao.at[others16], bs_sem, br_sem)
    back_all16.wait_send()
    back_all16.wait_recv()

    total = jnp.zeros((128, 1), jnp.float32)
    for n in range(4):
        cols = pl.ds(n * 512, 512)
        part = jnp.dot(rows[...], w[:, cols], preferred_element_type=jnp.float32)
        part = part + res_ref[:, cols].astype(jnp.float32)
        mixed[:, cols] = part
        total = total + jnp.sum(part * part, axis=1, keepdims=True)
    scale = lax.rsqrt(total / 2048.0 + norm_eps)
    normed[...] = (mixed[...] * scale * ngain_ref[...]).astype(jnp.bfloat16)

    def send_copy(k):
        return pltpu.make_async_remote_copy(
            src_ref=send.at[k, pl.ds(0, CAP)], dst_ref=recv.at[k, pl.ds(0, CAP)],
            send_sem=s_sem, recv_sem=r_sem.at[k // PER],
            device_id=shifted(me, k, 1), device_id_type=MESH)

    def send_block(first, count, sem):
        at = pl.ds(first, count)
        return pltpu.make_async_remote_copy(
            src_ref=send.at[at, pl.ds(0, CAP)], dst_ref=recv.at[at, pl.ds(0, CAP)],
            send_sem=s_sem, recv_sem=sem, device_id=(sp, dp), device_id_type=MESH)

    def pack(chunk, c):
        step = chunk * 16 + row // SLOT
        d = (step * 37) & 127
        z = (me[0] + (d >> 5)) & 3
        y = (me[1] + (d >> 3)) & 3
        x = (me[2] + (d >> 1)) & 3
        co = (me[3] + d) & 1
        dest = z * 32 + y * 8 + x * 2 + co
        rep = (dest == lane).astype(jnp.float32).astype(jnp.bfloat16)
        key = jnp.dot(rep, key_t, preferred_element_type=jnp.float32)
        on = key == (row & (SLOT - 1)).astype(jnp.float32)
        pick = jnp.where(on, 1.0, 0.0).astype(jnp.bfloat16)
        hi = jnp.dot(rep, gate_hi, preferred_element_type=jnp.float32)
        lo = jnp.dot(rep, gate_lo, preferred_element_type=jnp.float32)
        at = pl.ds(pl.multiple_of(chunk * 128, 128), 128)
        g_hi[at, :] = jnp.where(on, hi, 0.0).astype(jnp.bfloat16)
        g_lo[at, :] = jnp.where(on, lo, 0.0).astype(jnp.bfloat16)
        packed = jnp.dot(pick, normed[...], preferred_element_type=jnp.float32).astype(jnp.bfloat16)
        send[pl.ds(pl.multiple_of(chunk * 16, 16), 16)] = packed.reshape(16, SLOT, 2048)

        def start(i, c):
            send_copy((chunk - 1) * 16 + i).start()
            return c

        lax.fori_loop(jnp.where(chunk == 1, 1, 0), jnp.where(chunk == 0, 0, 16), start, 0)
        return c

    lax.fori_loop(0, 8, pack, 0)
    lax.fori_loop(112, 128, lambda k, c: (send_copy(k).start(), c)[1], 0)
    recv[0] = send[0]

    for c in loads[1:4]:
        c.wait()
    xs = normed[...]
    hidden = silu_mul(
        jnp.dot(xs, sg[...], preferred_element_type=jnp.float32),
        jnp.dot(xs, su[...], preferred_element_type=jnp.float32)).astype(jnp.bfloat16)
    for n in range(4):
        cols = pl.ds(n * 512, 512)
        mixed[:, cols] = mixed[:, cols] + jnp.dot(hidden, sd[:, cols], preferred_element_type=jnp.float32)

    for c in loads[4:]:
        c.wait()

    def back_copy(k):
        return pltpu.make_async_remote_copy(
            src_ref=fout.at[k, pl.ds(0, CAP)], dst_ref=ret.at[k, pl.ds(0, CAP)],
            send_sem=s2_sem, recv_sem=r2_sem,
            device_id=shifted(me, k, -1), device_id_type=MESH)

    def expert(g, c):
        first = g * PER
        lo = jnp.where(g == 0, 1, 0)

        @pl.when(g == 0)
        def _():
            send_block(1, PER - 1, r_sem.at[0]).wait_recv()

        @pl.when(g > 0)
        def _():
            send_block(pl.multiple_of(first, PER), PER, r_sem.at[g]).wait_recv()

        at = pl.ds(pl.multiple_of(first, PER), PER)
        x = recv[at].reshape(PER * SLOT, 2048)
        hid[...] = silu_mul(
            jnp.dot(x, eg[...], preferred_element_type=jnp.float32),
            jnp.dot(x, eu[...], preferred_element_type=jnp.float32)).astype(jnp.bfloat16)
        h = hid[...]
        for n in range(4):
            cols = pl.ds(n * 512, 512)
            o = jnp.dot(h, ed[:, cols], preferred_element_type=jnp.float32).astype(jnp.bfloat16)
            fout[at, :, cols] = o.reshape(PER, SLOT, 512)

        def reply(i, c):
            back_copy(first + i).start()
            return c

        lax.fori_loop(lo, PER, reply, 0)
        return c

    lax.fori_loop(0, GROUPS, expert, 0)

    ret[0, pl.ds(0, CAP)] = fout[0, pl.ds(0, CAP)]

    send_block(1, N_DEV - 1, r_sem.at[0]).wait_send()
    others = pl.ds(1, N_DEV - 1)
    back_all = pltpu.make_async_remote_copy(
        src_ref=fout.at[others, pl.ds(0, CAP)], dst_ref=ret.at[others, pl.ds(0, CAP)],
        send_sem=s2_sem, recv_sem=r2_sem, device_id=(sp, dp), device_id_type=MESH)
    back_all.wait_send()
    back_all.wait_recv()
    dims = (((0,), (0,)), ((), ()))
    for n in range(4):
        cols = pl.ds(n * 512, 512)
        r = ret[:, :, cols].reshape(N_DEV * SLOT, 512)
        routed = lax.dot_general(g_hi[...], r, dims, preferred_element_type=jnp.float32)
        routed = routed + lax.dot_general(g_lo[...], r, dims, preferred_element_type=jnp.float32)
        out_ref[:, cols] = (mixed[:, cols] + routed).astype(jnp.bfloat16)


def layer(*operands):
    bf, f32 = jnp.bfloat16, jnp.float32
    V, A = pl.BlockSpec(memory_space=pltpu.VMEM), pl.BlockSpec(memory_space=pl.ANY)
    S = pltpu.SemaphoreType.DMA
    M = pltpu.VMEM
    return pl.pallas_call(
        layer_kernel,
        out_shape=jax.ShapeDtypeStruct((128, 2048), bf),
        in_specs=[V, V, V, V, V, V, A, V, V, V, V, A, A, A, A, A, A],
        out_specs=V,
        scratch_shapes=[
            M((2048, 2048), bf),
            M((2048, 512), bf), M((2048, 512), bf), M((512, 2048), bf),
            M((2048, 512), bf), M((2048, 512), bf), M((512, 2048), bf),
            M((128, 2048), f32), M((128, 2048), bf),
            M((1024, 128), bf), M((1024, 128), bf),
            M((128, SLOT, 2048), bf), M((128, SLOT, 2048), bf),
            M((128, SLOT, 2048), bf), M((128, SLOT, 2048), bf),
            M((PER * SLOT, 512), bf),
            M((LEN, 128), f32), M((N_SP, 128, 128), bf), M((N_SP, 128, 128), bf), M((N_SP, 128, 128), bf),
            M((N_SP, 128, 128), bf), M((128, 2 * LEN), bf), M((2 * LEN, 256), bf), M((N_SP, 128, 128), bf),
            M((128, 2048), bf),
            S((7,)), S, S((GROUPS,)), S, S, S, S, S, S((BLOCKS,)), S, S, S, S((14,)),
        ],
        compiler_params=pltpu.CompilerParams(collective_id=0, has_side_effects=True, vmem_limit_bytes=63 * 2**20),
        name="layer",
    )(*operands)


def per_device(
    residual, query, key_value, out_weight, norm_gain, query_gain, key_gain, route_ids, route_weights,
    shared_gate, shared_up, shared_down, expert_gate, expert_up, expert_down,
):
    cosine, sine = rope_tables()
    combined = layer(
        query[0], key_value[0], jnp.asarray(cosine), jnp.asarray(sine), query_gain[None, :], key_gain[None, :],
        out_weight, residual[0], norm_gain[None, :], route_ids[0], route_weights[0],
        shared_gate, shared_up, shared_down, expert_gate, expert_up, expert_down,
    )
    return combined[None]


def solution(mesh):
    in_specs = (
        P("dp", "sp", None),
        P("dp", "sp", None, None),
        P("dp", "sp", None, None),
        P(None, "dp"),
        P(),
        P(),
        P(),
        P("dp", "sp", None),
        P("dp", "sp", None),
        P(),
        P(),
        P(),
        P(("sp", "dp"), None, None),
        P(("sp", "dp"), None, None),
        P(("sp", "dp"), None, None),
    )
    out_specs = P("dp", "sp", None)
    return jax.shard_map(
        per_device, mesh=mesh, in_specs=in_specs, out_specs=out_specs, check_vma=False
    )
```

time: 197 us -> 143 us (0.73)
  the two profiles are of different devices: /device:TPU:1 before, /device:TPU:19 now
where the time goes in v2:
time: 143 us
  Pallas kernels  138 us (97%)
  local copies, waits for them, and re-layouts  4.7 us (3%)
    pallas_call x1, Pallas kernels, layer(): pl.pallas_call(layer_kernel, out_shape=jax.ShapeDtypeStruct((128, 2048),...  138 us
    unnamed x3, local copies, waits for them, and re-layouts  4.7 us

profile of v2, /device:TPU:19, one launch (start us, length us, event | category | flops | bytes accessed | tf_op | source)
XLA Modules:
  0.0 142.8 jit_solution(6700998496714097947)
XLA Ops:
  0.0 1.4 copy.18
  1.4 1.4 copy.19
  2.8 138.1 %layer.1 = bf16[128,2048]{1,0:T(8,128)(2,1)} custom-call(bf16[128,16,128]{2,1,0:T(8,128)(2,1)} %bitcast.10, bf16[128,16,128]{2,1,0:T(8,128)(2,1)} %bitcast.11, f32[64,128]{1,0:T(8,128)} %constant.4.clone.cos_ref, f32[64,128]{1,0:T(8,128)} %constant.5.clone.sin_ref, f32[1,64]{1,0:T(1,128)} %bitcast.16, f32[1,64]{1,0:T(1,128)} %bitcast.17, ...), custom_call_target="tpu_custom_call" | custom-call | tf_op jit(solution)/shard_map/layer/pallas_call | solution.py:425
  140.9 1.9 %copy.21 = bf16[1,128,2048]{2,1,0:T(8,128)(2,1)} copy(bf16[1,128,2048]{2,1,0:T(8,128)(2,1)} %bitcast.9) | data formatting | bytes 1048576

commit v3 on v2

--- a/solution.py
+++ b/solution.py
@@ -19,6 +19,9 @@
 N_SP = 16
 LEN = 2048
 BLOCKS = 8
+HEADS = 4
+STRIDE = 91
+KEYS = 512
 EXP_SCALE = 0.125 * math.log2(math.e)
 
 
@@ -27,7 +30,7 @@
 
 
 def shifted(me_digits, k, sign):
-    d = lax.rem(k * 37, 128)
+    d = lax.rem(k * STRIDE, 128)
     out = []
     for m, v, size in zip(me_digits, digits(d), (4, 4, 4, 2)):
         out.append(lax.rem(m + sign * v + size, size))
@@ -58,8 +61,8 @@
     q_ref, kv_ref, cos_ref, sin_ref, qg_ref, kg_ref,
     w_ref, res_ref, ngain_ref, ids_ref, rw_ref, sg_ref, su_ref, sd_ref, eg_ref, eu_ref, ed_ref,
     out_ref,
-    w, sg, su, sd, eg, eu, ed, mixed, normed, g_hi, g_lo, send, recv, fout, ret, hid,
-    wide, sq, skv, rq, rkv, kt, vx, ao, rows,
+    w, sg, su, sd, eg, eu, ed, mixed, normed, g_hi, g_lo, pick, send, recv, fout, ret, hid,
+    wide, sq, skv, rq, rkv, kt, vx, ao, rows, s_even, s_odd, peak_even, peak_odd,
     ld_sem, s_sem, r_sem, s2_sem, r2_sem, kvs_sem, kvr_sem, qs_sem, qr_sem, bs_sem, br_sem, ws_sem, wr_sem,
 ):
     sp = lax.axis_index("sp")
@@ -77,11 +80,10 @@
         c.start()
     barrier = pltpu.get_barrier_semaphore()
 
-    def greet(k, c):
-        pl.semaphore_signal(barrier, inc=1, device_id=shifted(me, k, 1), device_id_type=MESH)
-        return c
-
-    lax.fori_loop(1, N_DEV, greet, 0)
+    sp_of = [((me[0] + i // 4) & 3) * 4 + ((me[1] + i % 4) & 3) for i in range(N_SP)]
+    dp_of = [((me[2] + i // 2) & 3) * 2 + ((me[3] + i % 2) & 1) for i in range(8)]
+    for i in range(1, N_DEV):
+        pl.semaphore_signal(barrier, inc=1, device_id=(sp_of[i // 8], dp_of[i % 8]), device_id_type=MESH)
 
     lane = lax.broadcasted_iota(jnp.int32, (128, 128), 1)
     row = lax.broadcasted_iota(jnp.int32, (128, 128), 0)
@@ -124,18 +126,22 @@
     def prepare_all(source, target, cos_gain, sin_gain, keep):
         wide[...] = source[...].astype(jnp.float32).reshape(LEN, 128)
 
-        def one(k, c):
-            x = wide[pl.ds(sp_shifted(me, k, 1), 128, stride=16), :]
+        def some(g, c):
+            x = jnp.concatenate(
+                [wide[pl.ds(sp_shifted(me, g * HEADS + i, 1), 128, stride=16), :] for i in range(HEADS)], axis=0)
             y = prepared(x, cos_gain, sin_gain)
             if keep:
-                y = jnp.where(lane < 64, y, x)
-            target[k] = y.astype(jnp.bfloat16)
+                y = jnp.where(jnp.broadcast_to(lane1 < 64, y.shape), y, x)
+            target[pl.ds(g * HEADS, HEADS)] = y.astype(jnp.bfloat16).reshape(HEADS, 128, 128)
             return c
 
-        lax.fori_loop(0, N_SP, one, 0)
-
-    prepare_all(kv_ref, skv, cosine * k_gain, sine * k_turn, True)
-    prepare_all(q_ref, sq, cosine * q_gain, sine * q_turn, False)
+        lax.fori_loop(0, N_SP // HEADS, some, 0)
+
+    def stacked(t):
+        return jnp.concatenate([t] * HEADS, axis=0)
+
+    prepare_all(kv_ref, skv, stacked(cosine * k_gain), stacked(sine * k_turn), True)
+    prepare_all(q_ref, sq, stacked(cosine * q_gain), stacked(sine * q_turn), False)
 
     pl.semaphore_wait(barrier, N_DEV - 1)
 
@@ -153,7 +159,6 @@
         return c
 
     lax.fori_loop(1, N_SP, send_kv, 0)
-    lax.fori_loop(1, N_SP, send_q, 0)
 
     loads[0].wait()
     x_at, core = me[2], me[3]
@@ -199,28 +204,46 @@
             device_id=(sp, dp), device_id_type=MESH).wait_send()
 
     raw = rw_ref[...]
-    gates = raw / jnp.sum(raw, axis=1, keepdims=True) * routed_scale
+    gates = raw / jnp.sum(raw, axis=0, keepdims=True) * routed_scale
     ids = ids_ref[...]
-    hit = jnp.zeros((128, 128), jnp.float32)
-    gate = jnp.zeros((128, 128), jnp.float32)
+    hit_t = jnp.zeros((128, 128), jnp.float32)
+    gate_t = jnp.zeros((128, 128), jnp.float32)
     for j in range(4):
-        on = ids[:, j : j + 1] == lane
-        hit = hit + jnp.where(on, 1.0, 0.0)
-        gate = gate + jnp.where(on, gates[:, j : j + 1], 0.0)
-    hit_t = jnp.transpose(hit)
-    gate_t = jnp.transpose(gate)
+        on = ids[j : j + 1, :] == row
+        hit_t = hit_t + jnp.where(on, 1.0, 0.0)
+        gate_t = gate_t + jnp.where(on, gates[j : j + 1, :], 0.0)
     before = (row < lane).astype(jnp.float32).astype(jnp.bfloat16)
     rank_t = jnp.dot(hit_t.astype(jnp.bfloat16), before, preferred_element_type=jnp.float32)
     key_t = jnp.where(hit_t > 0.0, rank_t, -1.0).astype(jnp.bfloat16)
     gate_hi = gate_t.astype(jnp.bfloat16)
     gate_lo = (gate_t - gate_hi.astype(jnp.float32)).astype(jnp.bfloat16)
 
+    table = jnp.concatenate([key_t, gate_hi, gate_lo], axis=1)
+    tall_row = lax.broadcasted_iota(jnp.int32, (256, 128), 0)
+    tall_lane = lax.broadcasted_iota(jnp.int32, (256, 128), 1)
+    for part in range(4):
+        d = ((part * 32 + tall_row // SLOT) * STRIDE) & 127
+        z = (me[0] + (d >> 5)) & 3
+        y = (me[1] + (d >> 3)) & 3
+        x = (me[2] + (d >> 1)) & 3
+        co = (me[3] + d) & 1
+        spread = (z * 32 + y * 8 + x * 2 + co == tall_lane).astype(jnp.float32).astype(jnp.bfloat16)
+        found = jnp.dot(spread, table, preferred_element_type=jnp.float32)
+        on = found[:, :128] == (tall_row & (SLOT - 1)).astype(jnp.float32)
+        at = pl.ds(part * 256, 256)
+        pick[at, :] = jnp.where(on, 1.0, 0.0).astype(jnp.bfloat16)
+        g_hi[at, :] = jnp.where(on, found[:, 128:256], 0.0).astype(jnp.bfloat16)
+        g_lo[at, :] = jnp.where(on, found[:, 256:], 0.0).astype(jnp.bfloat16)
+
     def clear(i, c):
         ret[pl.ds(pl.multiple_of(i * 16, 16), 16), pl.ds(CAP, SLOT - CAP)] = jnp.zeros((16, SLOT - CAP, 2048), jnp.bfloat16)
         return c
 
     lax.fori_loop(0, 8, clear, 0)
 
+    for h in range(2):
+        wanted = (lax.broadcasted_iota(jnp.int32, (LEN, 128), 1) < 64) == (h == 0)
+        vx[pl.ds(h * LEN, LEN), pl.ds(128, 128)] = jnp.where(wanted, 1.0, 0.0).astype(jnp.bfloat16)
     rkv[0] = skv[0]
     rq[0] = sq[0]
     others16 = pl.ds(1, N_SP - 1)
@@ -229,46 +252,70 @@
         return pltpu.make_async_remote_copy(
             src_ref=src, dst_ref=dst, send_sem=s, recv_sem=r, device_id=(sp, dp), device_id_type=MESH)
 
+    sp_all(skv.at[others16], rkv.at[others16], kvs_sem, kvr_sem).wait_send()
+    lax.fori_loop(1, N_SP, send_q, 0)
     sp_all(skv.at[others16], rkv.at[others16], kvs_sem, kvr_sem).wait_recv()
 
-    def lay(k, c):
-        pair = rkv[k].astype(jnp.float32)
-        swapped = pltpu.roll(pair, 64, 1)
-        low_lane = lane < 64
-        at = pl.ds(pl.multiple_of(k * 128, 128), 128)
-        at2 = pl.ds(pl.multiple_of(LEN + k * 128, 128), 128)
-        kt[:, at] = jnp.transpose(jnp.where(low_lane, pair, 0.0)).astype(jnp.bfloat16)
-        kt[:, at2] = jnp.transpose(jnp.where(low_lane, 0.0, swapped)).astype(jnp.bfloat16)
-        vx[at, pl.ds(0, 128)] = jnp.where(low_lane, swapped, 0.0).astype(jnp.bfloat16)
-        vx[at2, pl.ds(0, 128)] = jnp.where(low_lane, 0.0, pair).astype(jnp.bfloat16)
-        vx[at, pl.ds(128, 128)] = jnp.where(low_lane, 1.0, 0.0).astype(jnp.bfloat16)
-        vx[at2, pl.ds(128, 128)] = jnp.where(low_lane, 0.0, 1.0).astype(jnp.bfloat16)
-        return c
-
-    lax.fori_loop(0, N_SP, lay, 0)
+    low_lane = lane < 64
+
+    def lay(g, c):
+        for i in range(4):
+            k = g * 4 + i
+            pair = rkv[k].astype(jnp.float32)
+            flipped = jnp.transpose(pair)
+            top, none = flipped[0:64], jnp.zeros((64, 128), jnp.float32)
+            swapped = pltpu.roll(pair, 64, 1)
+            at = pl.ds(pl.multiple_of(k * 128, 128), 128)
+            at2 = pl.ds(pl.multiple_of(LEN + k * 128, 128), 128)
+            kt[:, at] = jnp.concatenate([top, none], axis=0).astype(jnp.bfloat16)
+            kt[:, at2] = jnp.concatenate([none, top], axis=0).astype(jnp.bfloat16)
+            vx[at, pl.ds(0, 128)] = jnp.where(low_lane, swapped, 0.0).astype(jnp.bfloat16)
+            vx[at2, pl.ds(0, 128)] = jnp.where(low_lane, 0.0, pair).astype(jnp.bfloat16)
+        return c
+
+    lax.fori_loop(0, N_SP // 4, lay, 0)
     own_rows = pl.ds(pl.multiple_of(sp * 128, 128), 128)
 
     def back_rows(k):
         return sp_copy(ao.at[k], rows.at[:, own_rows], k, -1, bs_sem, br_sem)
 
-    def block(b, c):
-        @pl.when(b == 0)
+    def scores(b, target, peaks):
+        q = rq[pl.ds(b * 2, 2)].reshape(256, 128)
+
+        def part(at, peak):
+            s = jnp.dot(q, kt[:, pl.ds(at, KEYS)], preferred_element_type=jnp.float32)
+            target[:, pl.ds(at, KEYS)] = s
+            for i in range(0, KEYS, 128):
+                peak = s[:, i : i + 128] if peak is None else jnp.maximum(peak, s[:, i : i + 128])
+            return peak
+
+        return part
+
+    sp_all(sq.at[1], rq.at[1], qs_sem, qr_sem.at[0]).wait_recv()
+    opening = scores(0, s_even, peak_even)
+    for h in range(2):
+        peak = None
+        for at in range(h * LEN, h * LEN + LEN, KEYS):
+            peak = opening(at, peak)
+        peak_even[:, pl.ds(h * 128, 128)] = peak
+
+    def block(b, held, held_peak, following, following_peak):
+        @pl.when(b < BLOCKS - 1)
         def _():
-            sp_all(sq.at[1], rq.at[1], qs_sem, qr_sem.at[0]).wait_recv()
-
-        @pl.when(b > 0)
-        def _():
-            two = pl.ds(b * 2, 2)
-            sp_all(sq.at[two], rq.at[two], qs_sem, qr_sem.at[b]).wait_recv()
-
-        q = rq[pl.ds(b * 2, 2)].reshape(256, 128)
-        o = jnp.zeros((256, 256), jnp.float32)
+            two = pl.ds(b * 2 + 2, 2)
+            sp_all(sq.at[two], rq.at[two], qs_sem, qr_sem.at[b + 1]).wait_recv()
+
+        part = scores(jnp.minimum(b + 1, BLOCKS - 1), following, following_peak)
+        o = None
         for h in range(2):
-            keys = pl.ds(h * LEN, LEN)
-            s = jnp.dot(q, kt[:, keys], preferred_element_type=jnp.float32)
-            top = jnp.max(s, axis=1, keepdims=True)
-            p = jnp.exp2((s - top) * EXP_SCALE).astype(jnp.bfloat16)
-            o = o + jnp.dot(p, vx[keys, :], preferred_element_type=jnp.float32)
+            top = jnp.max(held_peak[:, pl.ds(h * 128, 128)], axis=1, keepdims=True)
+            peak = None
+            for at in range(h * LEN, h * LEN + LEN, KEYS):
+                peak = part(at, peak)
+                p = jnp.exp2((held[:, pl.ds(at, KEYS)] - top) * EXP_SCALE).astype(jnp.bfloat16)
+                d = jnp.dot(p, vx[pl.ds(at, KEYS), :], preferred_element_type=jnp.float32)
+                o = d if o is None else o + d
+            following_peak[:, pl.ds(h * 128, 128)] = peak
         a = (o[:, :128] / o[:, 128:]).astype(jnp.bfloat16)
         ao[pl.ds(b * 2, 2)] = a.reshape(2, 128, 128)
 
@@ -278,15 +325,18 @@
 
         back_rows(b * 2 + 1).start()
 
-        @pl.when(b == 4)
+    def two_blocks(i, c):
+        block(i * 2, s_even, peak_even, s_odd, peak_odd)
+        block(i * 2 + 1, s_odd, peak_odd, s_even, peak_even)
+
+        @pl.when(i == 1)
         def _():
             w_relay()
 
         return c
 
-    lax.fori_loop(0, BLOCKS, block, 0)
+    lax.fori_loop(0, BLOCKS // 2, two_blocks, 0)
     rows[:, own_rows] = ao[0]
-    sp_all(skv.at[others16], rkv.at[others16], kvs_sem, kvr_sem).wait_send()
     sp_all(sq.at[others16], rq.at[others16], qs_sem, qr_sem.at[0]).wait_send()
     w_share(later)
     w_share(last)
@@ -318,23 +368,8 @@
             send_sem=s_sem, recv_sem=sem, device_id=(sp, dp), device_id_type=MESH)
 
     def pack(chunk, c):
-        step = chunk * 16 + row // SLOT
-        d = (step * 37) & 127
-        z = (me[0] + (d >> 5)) & 3
-        y = (me[1] + (d >> 3)) & 3
-        x = (me[2] + (d >> 1)) & 3
-        co = (me[3] + d) & 1
-        dest = z * 32 + y * 8 + x * 2 + co
-        rep = (dest == lane).astype(jnp.float32).astype(jnp.bfloat16)
-        key = jnp.dot(rep, key_t, preferred_element_type=jnp.float32)
-        on = key == (row & (SLOT - 1)).astype(jnp.float32)
-        pick = jnp.where(on, 1.0, 0.0).astype(jnp.bfloat16)
-        hi = jnp.dot(rep, gate_hi, preferred_element_type=jnp.float32)
-        lo = jnp.dot(rep, gate_lo, preferred_element_type=jnp.float32)
         at = pl.ds(pl.multiple_of(chunk * 128, 128), 128)
-        g_hi[at, :] = jnp.where(on, hi, 0.0).astype(jnp.bfloat16)
-        g_lo[at, :] = jnp.where(on, lo, 0.0).astype(jnp.bfloat16)
-        packed = jnp.dot(pick, normed[...], preferred_element_type=jnp.float32).astype(jnp.bfloat16)
+        packed = jnp.dot(pick[at, :], normed[...], preferred_element_type=jnp.float32).astype(jnp.bfloat16)
         send[pl.ds(pl.multiple_of(chunk * 16, 16), 16)] = packed.reshape(16, SLOT, 2048)
 
         def start(i, c):
@@ -432,13 +467,13 @@
             M((2048, 512), bf), M((2048, 512), bf), M((512, 2048), bf),
             M((2048, 512), bf), M((2048, 512), bf), M((512, 2048), bf),
             M((128, 2048), f32), M((128, 2048), bf),
-            M((1024, 128), bf), M((1024, 128), bf),
+            M((1024, 128), bf), M((1024, 128), bf), M((1024, 128), bf),
             M((128, SLOT, 2048), bf), M((128, SLOT, 2048), bf),
             M((128, SLOT, 2048), bf), M((128, SLOT, 2048), bf),
             M((PER * SLOT, 512), bf),
             M((LEN, 128), f32), M((N_SP, 128, 128), bf), M((N_SP, 128, 128), bf), M((N_SP, 128, 128), bf),
             M((N_SP, 128, 128), bf), M((128, 2 * LEN), bf), M((2 * LEN, 256), bf), M((N_SP, 128, 128), bf),
-            M((128, 2048), bf),
+            M((128, 2048), bf), M((256, 2 * LEN), f32), M((256, 2 * LEN), f32), M((256, 256), f32), M((256, 256), f32),
             S((7,)), S, S((GROUPS,)), S, S, S, S, S, S((BLOCKS,)), S, S, S, S((14,)),
         ],
         compiler_params=pltpu.CompilerParams(collective_id=0, has_side_effects=True, vmem_limit_bytes=63 * 2**20),
@@ -453,7 +488,7 @@
     cosine, sine = rope_tables()
     combined = layer(
         query[0], key_value[0], jnp.asarray(cosine), jnp.asarray(sine), query_gain[None, :], key_gain[None, :],
-        out_weight, residual[0], norm_gain[None, :], route_ids[0], route_weights[0],
+        out_weight, residual[0], norm_gain[None, :], route_ids[0].T, route_weights[0].T,
         shared_gate, shared_up, shared_down, expert_gate, expert_up, expert_down,
     )
     return combined[None]

time: 143 us -> 128 us (0.90)
  the two profiles are of different devices: /device:TPU:19 before, /device:TPU:1 now
where the time goes in v3:
time: 128 us; the launch traced here: 127 us
  Pallas kernels  126 us (98%)
  local copies, waits for them, and re-layouts  1.88 us (1%)
    pallas_call x1, Pallas kernels, layer(): pl.pallas_call(layer_kernel, out_shape=jax.ShapeDtypeStruct((128, 2048),...  126 us

profile of v3, /device:TPU:1, one launch (start us, length us, event | category | flops | bytes accessed | tf_op | source)
XLA Modules:
  0.0 127.4 jit_solution(163242517590606938)
XLA Ops:
  0.0 125.5 %layer.1 = bf16[128,2048]{1,0:T(8,128)(2,1)} custom-call(bf16[128,16,128]{2,1,0:T(8,128)(2,1)} %bitcast.14, bf16[128,16,128]{2,1,0:T(8,128)(2,1)} %bitcast.15, f32[64,128]{1,0:T(8,128)} %constant.4.clone.cos_ref, f32[64,128]{1,0:T(8,128)} %constant.5.clone.sin_ref, f32[1,64]{1,0:T(1,128)} %bitcast.20, f32[1,64]{1,0:T(1,128)} %bitcast.21, ...), custom_call_target="tpu_custom_call" | custom-call | tf_op jit(solution)/shard_map/layer/pallas_call | solution.py:460
  125.5 1.9 %copy.19 = bf16[1,128,2048]{2,1,0:T(8,128)(2,1)} copy(bf16[1,128,2048]{2,1,0:T(8,128)(2,1)} %bitcast.13) | data formatting | bytes 1048576

commit v4 on v3

--- a/solution.py
+++ b/solution.py
@@ -58,10 +58,10 @@
 
 
 def layer_kernel(
-    q_ref, kv_ref, cos_ref, sin_ref, qg_ref, kg_ref,
-    w_ref, res_ref, ngain_ref, ids_ref, rw_ref, sg_ref, su_ref, sd_ref, eg_ref, eu_ref, ed_ref,
+    q_hbm, kv_hbm, cos_ref, sin_ref, qg_ref, kg_ref,
+    w_ref, res_hbm, ngain_ref, ids_ref, rw_ref, sg_ref, su_ref, sd_ref, eg_ref, eu_ref, ed_ref,
     out_ref,
-    w, sg, su, sd, eg, eu, ed, mixed, normed, g_hi, g_lo, pick, send, recv, fout, ret, hid,
+    q_ref, kv_ref, res_ref, w, sg, su, sd, eg, eu, ed, mixed, normed, g_hi, g_lo, pick, send, recv, fout, ret, hid,
     wide, sq, skv, rq, rkv, kt, vx, ao, rows, s_even, s_odd, peak_even, peak_odd,
     ld_sem, s_sem, r_sem, s2_sem, r2_sem, kvs_sem, kvr_sem, qs_sem, qr_sem, bs_sem, br_sem, ws_sem, wr_sem,
 ):
@@ -73,7 +73,7 @@
     loads = [
         pltpu.make_async_copy(a, b, ld_sem.at[i])
         for i, (a, b) in enumerate(
-            [(w_ref, w.at[:, own_cols]), (sg_ref, sg), (su_ref, su), (sd_ref, sd), (eg_ref.at[0], eg), (eu_ref.at[0], eu), (ed_ref.at[0], ed)]
+            [(kv_hbm, kv_ref), (q_hbm, q_ref), (w_ref, w.at[:, own_cols]), (res_hbm, res_ref), (sg_ref, sg), (su_ref, su), (sd_ref, sd), (eg_ref.at[0], eg), (eu_ref.at[0], eu), (ed_ref.at[0], ed)]
         )
     ]
     for c in loads:
@@ -140,8 +140,8 @@
     def stacked(t):
         return jnp.concatenate([t] * HEADS, axis=0)
 
+    loads[0].wait()
     prepare_all(kv_ref, skv, stacked(cosine * k_gain), stacked(sine * k_turn), True)
-    prepare_all(q_ref, sq, stacked(cosine * q_gain), stacked(sine * q_turn), False)
 
     pl.semaphore_wait(barrier, N_DEV - 1)
 
@@ -160,48 +160,97 @@
 
     lax.fori_loop(1, N_SP, send_kv, 0)
 
-    loads[0].wait()
+    loads[2].wait()
     x_at, core = me[2], me[3]
-    right, left = lax.rem(x_at + 1, 4), lax.rem(x_at + 3, 4)
-
-    def w_copy(x_from, core_from, half, x_to, core_to, number):
-        size = LEN if half is None else LEN // 2
-        at = w.at[pl.ds(0 if half is None else half * size, size), pl.ds(pl.multiple_of((x_from * 2 + core_from) * 256, 256), 256)]
+    right, left, far = lax.rem(x_at + 1, 4), lax.rem(x_at + 3, 4), lax.rem(x_at + 2, 4)
+    HALF, SUB = 512, 128
+
+    def w_copy(first, size, x_from, device, number):
+        at = w.at[pl.ds(first, size), pl.ds(pl.multiple_of((x_from * 2 + core) * 256, 256), 256)]
         return pltpu.make_async_remote_copy(
             src_ref=at, dst_ref=at, send_sem=ws_sem, recv_sem=wr_sem.at[number],
-            device_id=(sp, x_to * 2 + core_to), device_id_type=MESH)
-
-    w_copy(x_at, core, 0, right, core, 0).start()
-    w_copy(x_at, core, 1, left, core, 1).start()
-    w_copy(x_at, core, 1, right, core, 2).start()
-    w_copy(x_at, core, 0, left, core, 3).start()
-    w_copy(x_at, core, None, x_at, 1 - core, 4).start()
-    far = lax.rem(x_at + 2, 4)
-    early = ((left, 0, 0), (right, 1, 1))
-    later = ((left, 1, 2), (right, 0, 3))
-    last = ((far, 0, 5), (far, 1, 6))
+            device_id=device, device_id_type=MESH)
+
+    def w_wait(rows, columns, number):
+        at = w.at[pl.ds(0, rows), pl.ds(0, columns)]
+        pltpu.make_async_remote_copy(
+            src_ref=at, dst_ref=at, send_sem=ws_sem, recv_sem=wr_sem.at[number],
+            device_id=(sp, dp), device_id_type=MESH).wait_recv()
+
+    def along_x(x_to):
+        return (sp, x_to * 2 + core)
+
+    other_core = (sp, x_at * 2 + 1 - core)
+    y_sub = pl.multiple_of(1024 + me[1] * SUB, SUB)
+    z_sub = pl.multiple_of(1536 + me[0] * SUB, SUB)
+    for x_to in (right, left, far):
+        w_copy(y_sub, SUB, x_at, along_x(x_to), 0).start()
+        w_copy(z_sub, SUB, x_at, along_x(x_to), 0).start()
+    w_copy(0, HALF, x_at, along_x(right), 1).start()
+    w_copy(HALF, HALF, x_at, along_x(left), 2).start()
+    w_copy(HALF, HALF, x_at, along_x(right), 3).start()
+    w_copy(0, HALF, x_at, along_x(left), 4).start()
+    w_copy(0, LEN, x_at, other_core, 7).start()
+
+    def y_sub_of(step):
+        return pl.multiple_of(1024 + lax.rem(me[1] + step, 4) * SUB, SUB)
+
+    def z_sub_of(step):
+        return pl.multiple_of(1536 + lax.rem(me[0] + step, 4) * SUB, SUB)
+
+    def w_lines():
+        w_wait(6 * SUB, 256, 0)
+        for step in range(1, 4):
+            y_to, z_to = lax.rem(me[1] + step, 4), lax.rem(me[0] + step, 4)
+            for x_from in (right, left, far):
+                w_copy(y_sub, SUB, x_from, (me[0] * 4 + y_to, dp), 16 + step).start()
+                w_copy(z_sub, SUB, x_from, (z_to * 4 + me[1], dp), 19 + step).start()
+        for x_from in (right, left, far):
+            w_copy(y_sub, SUB, x_from, other_core, 5).start()
+            w_copy(z_sub, SUB, x_from, other_core, 5).start()
 
     def w_relay():
-        for x_from, half, number in early:
-            w_copy(x_from, core, half, right, core, number).wait_recv()
-        w_copy(left, core, 0, right, core, 5).start()
-        w_copy(right, core, 1, left, core, 6).start()
-        for x_from, half, number in early:
-            w_copy(x_from, core, half, x_at, 1 - core, 7 + number).start()
-
-    def w_share(some):
-        for x_from, half, number in some:
-            w_copy(x_from, core, half, right, core, number).wait_recv()
-            w_copy(x_from, core, half, x_at, 1 - core, 7 + number).start()
+        w_wait(HALF, 256, 1)
+        w_wait(HALF, 256, 2)
+        w_copy(0, HALF, left, along_x(right), 8).start()
+        w_copy(HALF, HALF, right, along_x(left), 9).start()
+        w_copy(0, HALF, left, other_core, 10).start()
+        w_copy(HALF, HALF, right, other_core, 11).start()
+
+    def w_later():
+        w_wait(HALF, 256, 3)
+        w_wait(HALF, 256, 4)
+        w_copy(HALF, HALF, left, other_core, 12).start()
+        w_copy(0, HALF, right, other_core, 13).start()
 
     def w_finish():
-        w_copy(x_at, 1 - core, None, x_at, core, 4).wait_recv()
-        for x_from, half, number in early + later + last:
-            w_copy(x_from, 1 - core, half, x_at, core, 7 + number).wait_recv()
+        for step in range(1, 4):
+            w_wait(3 * SUB, 256, 16 + step)
+            for x_from in (right, left, far):
+                w_copy(y_sub_of(4 - step), SUB, x_from, other_core, 14).start()
+            w_wait(3 * SUB, 256, 19 + step)
+            for x_from in (right, left, far):
+                w_copy(z_sub_of(4 - step), SUB, x_from, other_core, 14).start()
+        w_wait(HALF, 256, 8)
+        w_copy(0, HALF, far, other_core, 15).start()
+        w_wait(HALF, 256, 9)
+        w_copy(HALF, HALF, far, other_core, 16).start()
+        w_wait(LEN, 256, 7)
+        for number in range(10, 14):
+            w_wait(HALF, 256, number)
+        w_wait(6 * SUB, 256, 5)
+        w_wait(9 * SUB, 512, 14)
+        w_wait(HALF, 256, 15)
+        w_wait(HALF, 256, 16)
+
+    def w_sent():
         everything = w.at[:, pl.ds(0, 7 * 256)]
         pltpu.make_async_remote_copy(
             src_ref=everything, dst_ref=everything, send_sem=ws_sem, recv_sem=wr_sem.at[0],
             device_id=(sp, dp), device_id_type=MESH).wait_send()
+
+    loads[1].wait()
+    prepare_all(q_ref, sq, stacked(cosine * q_gain), stacked(sine * q_turn), False)
 
     raw = rw_ref[...]
     gates = raw / jnp.sum(raw, axis=0, keepdims=True) * routed_scale
@@ -327,24 +376,31 @@
 
     def two_blocks(i, c):
         block(i * 2, s_even, peak_even, s_odd, peak_odd)
+        @pl.when(i == 0)
+        def _():
+            w_lines()
+
         block(i * 2 + 1, s_odd, peak_odd, s_even, peak_even)
 
         @pl.when(i == 1)
         def _():
             w_relay()
+
+        @pl.when(i == 2)
+        def _():
+            w_later()
 
         return c
 
     lax.fori_loop(0, BLOCKS // 2, two_blocks, 0)
     rows[:, own_rows] = ao[0]
     sp_all(sq.at[others16], rq.at[others16], qs_sem, qr_sem.at[0]).wait_send()
-    w_share(later)
-    w_share(last)
     w_finish()
     back_all16 = sp_all(ao.at[others16], ao.at[others16], bs_sem, br_sem)
     back_all16.wait_send()
     back_all16.wait_recv()
 
+    loads[3].wait()
     total = jnp.zeros((128, 1), jnp.float32)
     for n in range(4):
         cols = pl.ds(n * 512, 512)
@@ -383,7 +439,7 @@
     lax.fori_loop(112, 128, lambda k, c: (send_copy(k).start(), c)[1], 0)
     recv[0] = send[0]
 
-    for c in loads[1:4]:
+    for c in loads[4:7]:
         c.wait()
     xs = normed[...]
     hidden = silu_mul(
@@ -393,13 +449,13 @@
         cols = pl.ds(n * 512, 512)
         mixed[:, cols] = mixed[:, cols] + jnp.dot(hidden, sd[:, cols], preferred_element_type=jnp.float32)
 
-    for c in loads[4:]:
+    for c in loads[7:]:
         c.wait()
 
     def back_copy(k):
         return pltpu.make_async_remote_copy(
             src_ref=fout.at[k, pl.ds(0, CAP)], dst_ref=ret.at[k, pl.ds(0, CAP)],
-            send_sem=s2_sem, recv_sem=r2_sem,
+            send_sem=s2_sem, recv_sem=r2_sem.at[k // PER],
             device_id=shifted(me, k, -1), device_id_type=MESH)
 
     def expert(g, c):
@@ -436,20 +492,29 @@
 
     ret[0, pl.ds(0, CAP)] = fout[0, pl.ds(0, CAP)]
 
+    def back_block(first, count, number):
+        at = pl.ds(first, count)
+        return pltpu.make_async_remote_copy(
+            src_ref=fout.at[at, pl.ds(0, CAP)], dst_ref=ret.at[at, pl.ds(0, CAP)],
+            send_sem=s2_sem, recv_sem=r2_sem.at[number], device_id=(sp, dp), device_id_type=MESH)
+
+    w_sent()
     send_block(1, N_DEV - 1, r_sem.at[0]).wait_send()
-    others = pl.ds(1, N_DEV - 1)
-    back_all = pltpu.make_async_remote_copy(
-        src_ref=fout.at[others, pl.ds(0, CAP)], dst_ref=ret.at[others, pl.ds(0, CAP)],
-        send_sem=s2_sem, recv_sem=r2_sem, device_id=(sp, dp), device_id_type=MESH)
-    back_all.wait_send()
-    back_all.wait_recv()
     dims = (((0,), (0,)), ((), ()))
-    for n in range(4):
-        cols = pl.ds(n * 512, 512)
-        r = ret[:, :, cols].reshape(N_DEV * SLOT, 512)
-        routed = lax.dot_general(g_hi[...], r, dims, preferred_element_type=jnp.float32)
-        routed = routed + lax.dot_general(g_lo[...], r, dims, preferred_element_type=jnp.float32)
-        out_ref[:, cols] = (mixed[:, cols] + routed).astype(jnp.bfloat16)
+    for g in range(GROUPS):
+        first = max(1, g * PER)
+        back_block(first, (g + 1) * PER - first, g).wait_recv()
+        at = pl.ds(g * PER * SLOT, PER * SLOT)
+        for n in range(4):
+            cols = pl.ds(n * 512, 512)
+            r = ret[pl.ds(g * PER, PER), :, cols].reshape(PER * SLOT, 512)
+            routed = lax.dot_general(g_hi[at, :], r, dims, preferred_element_type=jnp.float32)
+            routed = routed + lax.dot_general(g_lo[at, :], r, dims, preferred_element_type=jnp.float32)
+            if g < GROUPS - 1:
+                mixed[:, cols] = mixed[:, cols] + routed
+            else:
+                out_ref[:, cols] = (mixed[:, cols] + routed).astype(jnp.bfloat16)
+    back_block(1, N_DEV - 1, 0).wait_send()
 
 
 def layer(*operands):
@@ -460,9 +525,10 @@
     return pl.pallas_call(
         layer_kernel,
         out_shape=jax.ShapeDtypeStruct((128, 2048), bf),
-        in_specs=[V, V, V, V, V, V, A, V, V, V, V, A, A, A, A, A, A],
+        in_specs=[A, A, V, V, V, V, A, A, V, V, V, A, A, A, A, A, A],
         out_specs=V,
         scratch_shapes=[
+            M((128, 16, 128), bf), M((128, 16, 128), bf), M((128, 2048), bf),
             M((2048, 2048), bf),
             M((2048, 512), bf), M((2048, 512), bf), M((512, 2048), bf),
             M((2048, 512), bf), M((2048, 512), bf), M((512, 2048), bf),
@@ -474,7 +540,7 @@
             M((LEN, 128), f32), M((N_SP, 128, 128), bf), M((N_SP, 128, 128), bf), M((N_SP, 128, 128), bf),
             M((N_SP, 128, 128), bf), M((128, 2 * LEN), bf), M((2 * LEN, 256), bf), M((N_SP, 128, 128), bf),
             M((128, 2048), bf), M((256, 2 * LEN), f32), M((256, 2 * LEN), f32), M((256, 256), f32), M((256, 256), f32),
-            S((7,)), S, S((GROUPS,)), S, S, S, S, S, S((BLOCKS,)), S, S, S, S((14,)),
+            S((10,)), S, S((GROUPS,)), S, S((GROUPS,)), S, S, S, S((BLOCKS,)), S, S, S, S((23,)),
         ],
         compiler_params=pltpu.CompilerParams(collective_id=0, has_side_effects=True, vmem_limit_bytes=63 * 2**20),
         name="layer",

time: 128 us -> 116 us (0.906)
  Pallas kernels: 126 us -> 114 us
    pallas_call x1, Pallas kernels: 126 us -> 114 us  [layer(): pl.pallas_call(layer_kernel, out_shape=jax.ShapeDtypeStruct((128, 2048),...]
where the time goes in v4:
time: 116 us
  Pallas kernels  114 us (98%)
  local copies, waits for them, and re-layouts  1.88 us (2%)
    pallas_call x1, Pallas kernels, layer(): pl.pallas_call(layer_kernel, out_shape=jax.ShapeDtypeStruct((128, 2048),...  114 us

profile of v4, /device:TPU:1, one launch (start us, length us, event | category | flops | bytes accessed | tf_op | source)
XLA Modules:
  0.0 115.9 jit_solution(11677364348925451009)
XLA Ops:
  0.0 114.0 %layer.1 = bf16[128,2048]{1,0:T(8,128)(2,1)} custom-call(bf16[128,16,128]{2,1,0:T(8,128)(2,1)} %bitcast.14, bf16[128,16,128]{2,1,0:T(8,128)(2,1)} %bitcast.15, f32[64,128]{1,0:T(8,128)} %constant.4.clone.cos_ref, f32[64,128]{1,0:T(8,128)} %constant.5.clone.sin_ref, f32[1,64]{1,0:T(1,128)} %bitcast.20, f32[1,64]{1,0:T(1,128)} %bitcast.21, ...), custom_call_target="tpu_custom_call" | custom-call | tf_op jit(solution)/shard_map/layer/pallas_call | solution.py:525
  114.0 1.9 %copy.19 = bf16[1,128,2048]{2,1,0:T(8,128)(2,1)} copy(bf16[1,128,2048]{2,1,0:T(8,128)(2,1)} %bitcast.13) | data formatting | bytes 1048576

commit v5 on v4

--- a/solution.py
+++ b/solution.py
@@ -63,7 +63,7 @@
     out_ref,
     q_ref, kv_ref, res_ref, w, sg, su, sd, eg, eu, ed, mixed, normed, g_hi, g_lo, pick, send, recv, fout, ret, hid,
     wide, sq, skv, rq, rkv, kt, vx, ao, rows, s_even, s_odd, peak_even, peak_odd,
-    ld_sem, s_sem, r_sem, s2_sem, r2_sem, kvs_sem, kvr_sem, qs_sem, qr_sem, bs_sem, br_sem, ws_sem, wr_sem,
+    ld_sem, s_sem, r_sem, s2_sem, r2_sem, kvs_sem, kvr_sem, qs_sem, qr_sem, bs_sem, br_sem, ws_sem, wr_sem, all_sem,
 ):
     sp = lax.axis_index("sp")
     dp = lax.axis_index("dp")
@@ -76,14 +76,16 @@
             [(kv_hbm, kv_ref), (q_hbm, q_ref), (w_ref, w.at[:, own_cols]), (res_hbm, res_ref), (sg_ref, sg), (su_ref, su), (sd_ref, sd), (eg_ref.at[0], eg), (eu_ref.at[0], eu), (ed_ref.at[0], ed)]
         )
     ]
-    for c in loads:
+    for c in loads[:3]:
         c.start()
     barrier = pltpu.get_barrier_semaphore()
 
     sp_of = [((me[0] + i // 4) & 3) * 4 + ((me[1] + i % 4) & 3) for i in range(N_SP)]
     dp_of = [((me[2] + i // 2) & 3) * 2 + ((me[3] + i % 2) & 1) for i in range(8)]
-    for i in range(1, N_DEV):
-        pl.semaphore_signal(barrier, inc=1, device_id=(sp_of[i // 8], dp_of[i % 8]), device_id_type=MESH)
+    for i in range(1, N_SP):
+        pl.semaphore_signal(barrier, inc=1, device_id=(sp_of[i], dp), device_id_type=MESH)
+    for i in range(1, 8):
+        pl.semaphore_signal(barrier, inc=1, device_id=(sp, dp_of[i]), device_id_type=MESH)
 
     lane = lax.broadcasted_iota(jnp.int32, (128, 128), 1)
     row = lax.broadcasted_iota(jnp.int32, (128, 128), 0)
@@ -143,7 +145,9 @@
     loads[0].wait()
     prepare_all(kv_ref, skv, stacked(cosine * k_gain), stacked(sine * k_turn), True)
 
-    pl.semaphore_wait(barrier, N_DEV - 1)
+    pl.semaphore_wait(barrier, N_SP - 1 + 7)
+    for i in range(1, 8):
+        pl.semaphore_signal(all_sem, inc=1, device_id=(sp, dp_of[i]), device_id_type=MESH)
 
     def sp_copy(src, dst, k, sign, s, r):
         return pltpu.make_async_remote_copy(
@@ -163,7 +167,8 @@
     loads[2].wait()
     x_at, core = me[2], me[3]
     right, left, far = lax.rem(x_at + 1, 4), lax.rem(x_at + 3, 4), lax.rem(x_at + 2, 4)
-    HALF, SUB = 512, 128
+    HALF, SUB = 576, 112
+    Y_ROWS, Z_ROWS = 2 * HALF, 2 * HALF + 4 * SUB
 
     def w_copy(first, size, x_from, device, number):
         at = w.at[pl.ds(first, size), pl.ds(pl.multiple_of((x_from * 2 + core) * 256, 256), 256)]
@@ -181,8 +186,8 @@
         return (sp, x_to * 2 + core)
 
     other_core = (sp, x_at * 2 + 1 - core)
-    y_sub = pl.multiple_of(1024 + me[1] * SUB, SUB)
-    z_sub = pl.multiple_of(1536 + me[0] * SUB, SUB)
+    y_sub = pl.multiple_of(Y_ROWS + me[1] * SUB, 16)
+    z_sub = pl.multiple_of(Z_ROWS + me[0] * SUB, 16)
     for x_to in (right, left, far):
         w_copy(y_sub, SUB, x_at, along_x(x_to), 0).start()
         w_copy(z_sub, SUB, x_at, along_x(x_to), 0).start()
@@ -191,12 +196,14 @@
     w_copy(HALF, HALF, x_at, along_x(right), 3).start()
     w_copy(0, HALF, x_at, along_x(left), 4).start()
     w_copy(0, LEN, x_at, other_core, 7).start()
+    for c in loads[3:]:
+        c.start()
 
     def y_sub_of(step):
-        return pl.multiple_of(1024 + lax.rem(me[1] + step, 4) * SUB, SUB)
+        return pl.multiple_of(Y_ROWS + lax.rem(me[1] + step, 4) * SUB, 16)
 
     def z_sub_of(step):
-        return pl.multiple_of(1536 + lax.rem(me[0] + step, 4) * SUB, SUB)
+        return pl.multiple_of(Z_ROWS + lax.rem(me[0] + step, 4) * SUB, 16)
 
     def w_lines():
         w_wait(6 * SUB, 256, 0)
@@ -411,6 +418,8 @@
     scale = lax.rsqrt(total / 2048.0 + norm_eps)
     normed[...] = (mixed[...] * scale * ngain_ref[...]).astype(jnp.bfloat16)
 
+    pl.semaphore_wait(all_sem, 7)
+
     def send_copy(k):
         return pltpu.make_async_remote_copy(
             src_ref=send.at[k, pl.ds(0, CAP)], dst_ref=recv.at[k, pl.ds(0, CAP)],
@@ -524,7 +533,7 @@
     M = pltpu.VMEM
     return pl.pallas_call(
         layer_kernel,
-        out_shape=jax.ShapeDtypeStruct((128, 2048), bf),
+        out_shape=pltpu.VMEM((128, 2048), bf),
         in_specs=[A, A, V, V, V, V, A, A, V, V, V, A, A, A, A, A, A],
         out_specs=V,
         scratch_shapes=[
@@ -540,7 +549,7 @@
             M((LEN, 128), f32), M((N_SP, 128, 128), bf), M((N_SP, 128, 128), bf), M((N_SP, 128, 128), bf),
             M((N_SP, 128, 128), bf), M((128, 2 * LEN), bf), M((2 * LEN, 256), bf), M((N_SP, 128, 128), bf),
             M((128, 2048), bf), M((256, 2 * LEN), f32), M((256, 2 * LEN), f32), M((256, 256), f32), M((256, 256), f32),
-            S((10,)), S, S((GROUPS,)), S, S((GROUPS,)), S, S, S, S((BLOCKS,)), S, S, S, S((23,)),
+            S((10,)), S, S((GROUPS,)), S, S((GROUPS,)), S, S, S, S((BLOCKS,)), S, S, S, S((23,)), pltpu.SemaphoreType.REGULAR,
         ],
         compiler_params=pltpu.CompilerParams(collective_id=0, has_side_effects=True, vmem_limit_bytes=63 * 2**20),
         name="layer",

time: 116 us -> 111 us (0.957)
  Pallas kernels: 114 us -> 110 us
    pallas_call x1, Pallas kernels: 114 us -> 110 us  [layer(): pl.pallas_call(layer_kernel, out_shape=pltpu.VMEM((128, 2048), bf), in_sp...]
where the time goes in v5:
time: 111 us
  Pallas kernels  110 us (99%)
    pallas_call x1, Pallas kernels, layer(): pl.pallas_call(layer_kernel, out_shape=pltpu.VMEM((128, 2048), bf), in_sp...  110 us

profile of v5, /device:TPU:1, one launch (start us, length us, event | category | flops | bytes accessed | tf_op | source)
XLA Modules:
  0.0 111.3 jit_solution(6754689505450784804)
XLA Ops:
  0.0 110.5 %layer.1 = bf16[128,2048]{1,0:T(8,128)(2,1)S(1)} custom-call(bf16[128,16,128]{2,1,0:T(8,128)(2,1)} %bitcast.14, bf16[128,16,128]{2,1,0:T(8,128)(2,1)} %bitcast.15, f32[64,128]{1,0:T(8,128)} %constant.4.clone.cos_ref, f32[64,128]{1,0:T(8,128)} %constant.5.clone.sin_ref, f32[1,64]{1,0:T(1,128)} %bitcast.20, f32[1,64]{1,0:T(1,128)} %bitcast.21, ...), custom_call_target="tpu_custom_call" | custom-call | tf_op jit(solution)/shard_map/layer/pallas_call | solution.py:534
  110.5 0.8 copy.19

commit v6 on v5

--- a/solution.py
+++ b/solution.py
@@ -20,7 +20,7 @@
 LEN = 2048
 BLOCKS = 8
 HEADS = 4
-STRIDE = 91
+STRIDE = 101
 KEYS = 512
 EXP_SCALE = 0.125 * math.log2(math.e)
 

time: 111 us -> 113 us (1.018)
  Pallas kernels: 110 us -> 112 us
    pallas_call x1, Pallas kernels: 110 us -> 112 us  [layer(): pl.pallas_call(layer_kernel, out_shape=pltpu.VMEM((128, 2048), bf), in_sp...]
where the time goes in v6:
time: 113 us
  Pallas kernels  112 us (99%)
    pallas_call x1, Pallas kernels, layer(): pl.pallas_call(layer_kernel, out_shape=pltpu.VMEM((128, 2048), bf), in_sp...  112 us

profile of v6, /device:TPU:1, one launch (start us, length us, event | category | flops | bytes accessed | tf_op | source)
XLA Modules:
  0.0 112.8 jit_solution(13150358866736391929)
XLA Ops:
  0.0 112.0 %layer.1 = bf16[128,2048]{1,0:T(8,128)(2,1)S(1)} custom-call(bf16[128,16,128]{2,1,0:T(8,128)(2,1)} %bitcast.14, bf16[128,16,128]{2,1,0:T(8,128)(2,1)} %bitcast.15, f32[64,128]{1,0:T(8,128)} %constant.4.clone.cos_ref, f32[64,128]{1,0:T(8,128)} %constant.5.clone.sin_ref, f32[1,64]{1,0:T(1,128)} %bitcast.20, f32[1,64]{1,0:T(1,128)} %bitcast.21, ...), custom_call_target="tpu_custom_call" | custom-call | tf_op jit(solution)/shard_map/layer/pallas_call | solution.py:534
  112.0 0.8 copy.19
